TPU v7x, 32 devices: a whole 2x2x4 slice. The times are simulated.
32 devices in a mesh: ra: 8 (over z, x), cb: 4 (over y, core).
Axes of the slice: x: 2, y: 2, z: 4, core: 2. Of those that a mesh axis runs over, the one named last changes fastest.
Arguments:
- inputs: bfloat16 [1536, 4096], P(None, 'ra'), may hold values from -12 to 12
- gate_weight: bfloat16 [2, 4096, 11264], P(None, 'ra', 'cb'), may hold values from -0.09375 to 0.09375
- up_weight: bfloat16 [2, 4096, 11264], P(None, 'ra', 'cb'), may hold values from -0.09375 to 0.09375
- down_weight: bfloat16 [2, 11264, 4096], P(None, 'cb', 'ra'), may hold values from -0.0546875 to 0.0546875
- norm_gain: float32 [2, 4096], P(None, 'ra'), may hold values from 0.05 to 8
- norm_shift: float32 [2, 4096], P(None, 'ra'), may hold values from -1.5 to 1.5
Outputs:
- outputs: bfloat16 [1536, 4096], P(None, 'ra')
All inputs are finite; a program needn't handle non-finite values.
Results may differ from a plain program's by a relative error of at most 0.04.
Values may be sent and summed in bfloat16 or wider, within the bound.
A program may use at most 128 MiB of HBM per device.

v0:
```python
import jax
import jax.numpy as jnp
from jax import lax
from jax.sharding import PartitionSpec as P

LAYERS = 2
RESIDUAL = 0.5
EPSILON = 1e-05
PAIR = 2
TOKEN_CHUNKS = 3
COLUMN_CHUNKS = 2
BF16 = jnp.bfloat16
F32 = jnp.float32


def dot(a, b):
    return jnp.dot(a, b, preferred_element_type=F32)


def axis_ring(total, stride, size):
    perm = []
    for i in range(total):
        at = (i // stride) % size
        perm.append((i, i + (((at + 1) % size) - at) * stride))
    return perm


def xor_perm(total, bit):
    return [(i, i ^ bit) for i in range(total)]


def swap(x, axis):
    return lax.ppermute(x, axis, xor_perm(lax.axis_size(axis), 1))


def part(x, at, size, dim=0):
    return lax.dynamic_slice_in_dim(x, at * size, size, dim)


def ring_reduce(block, axis, stride, size, me):
    perm = axis_ring(lax.axis_size(axis), stride, size)
    total = block(lax.rem(me + size - 1, size))
    for step in range(1, size):
        arrived = lax.ppermute(total.astype(BF16), axis, perm)
        total = arrived.astype(F32) + block(lax.rem(me + 2 * size - 1 - step, size))
    return total


def ring_gather(x, axis, stride, size, me):
    perm = axis_ring(lax.axis_size(axis), stride, size)
    rows = x.shape[0]
    whole = jnp.zeros((rows * size,) + x.shape[1:], x.dtype)
    whole = lax.dynamic_update_slice_in_dim(whole, x, me * rows, 0)
    for step in range(1, size):
        x = lax.ppermute(x, axis, perm)
        owner = lax.rem(me + size - step, size)
        whole = lax.dynamic_update_slice_in_dim(whole, x, owner * rows, 0)
    return whole


def swap_gather(x, axis, me):
    other = swap(x, axis)
    first = jnp.where(me == 0, x, other)
    second = jnp.where(me == 0, other, x)
    return jnp.concatenate((first, second), axis=0)


def sum_over_ra(stats):
    total = lax.axis_size("ra")
    if total & (total - 1):
        return lax.psum(stats, "ra")
    bit = 1
    while bit < total:
        stats = stats + lax.ppermute(stats, "ra", xor_perm(total, bit))
        bit *= 2
    return stats


def cuts_of(width):
    step = -(-width // COLUMN_CHUNKS)
    step = min(width, -(-step // 128) * 128)
    return [(s, min(step, width - s)) for s in range(0, width, step)]


def per_device(inputs, gate_weight, up_weight, down_weight, norm_gain, norm_shift):
    ra, cb = lax.axis_size("ra"), lax.axis_size("cb")
    r, c = lax.axis_index("ra"), lax.axis_index("cb")
    groups, rows_y = ra // PAIR, cb // 2
    q, g = lax.rem(r, PAIR), r // PAIR
    core, y = lax.rem(c, 2), c // 2
    tokens, width = inputs.shape
    full_width = width * ra
    columns = gate_weight.shape[2]
    half = columns // PAIR
    cuts = cuts_of(half)
    chunk = tokens // TOKEN_CHUNKS

    queue = [None]

    def queued_swap(away):
        if queue[0] is not None:
            away, queue[0] = lax.optimization_barrier((away, queue[0]))
        queue[0] = swap(away, "ra")
        return queue[0]

    def weights_of(layer):
        kept, sent = q * half, (1 - q) * half
        pairs, downs = [], []
        for start, size in cuts:
            own = jnp.concatenate(
                [lax.dynamic_slice(w, (layer, 0, kept + start), (1, width, size))[0] for w in (gate_weight, up_weight)], axis=1
            )
            away = jnp.concatenate(
                [lax.dynamic_slice(w, (layer, 0, sent + start), (1, width, size))[0] for w in (gate_weight, up_weight)], axis=1
            )
            pairs.append((own, queued_swap(away)))
        for start, size in cuts:
            own = lax.dynamic_slice(down_weight, (layer, kept + start, 0), (1, size, width))[0]
            away = lax.dynamic_slice(down_weight, (layer, sent + start, 0), (1, size, width))[0]
            downs.append((own, queued_swap(away)))
        return pairs, downs

    streams = []
    for k in range(TOKEN_CHUNKS):
        own = inputs[k * chunk:(k + 1) * chunk]
        over = swap(part(own, core, chunk // 2), "ra")
        streams.append((own, swap_gather(over, "cb", core)))

    gate_open = None
    for layer in range(LAYERS):
        pairs, downs = weights_of(layer)
        last = layer == LAYERS - 1
        after = []
        for own, other in streams:
            block_rows = chunk // groups
            outs_own, outs_other = 0.0, 0.0
            if gate_open is not None:
                own, other, _ = lax.optimization_barrier((own, other, gate_open))
            opened = []
            for (w_own, w_other), (d_own, d_other) in zip(pairs, downs):
                size = d_own.shape[0]

                def block(at):
                    return dot(part(own, at, block_rows), w_own) + dot(part(other, at, block_rows), w_other)

                total = ring_reduce(block, "ra", PAIR, groups, g)
                hidden = (jax.nn.silu(total[:, :size]) * total[:, size:]).astype(BF16)
                opened.append(hidden)
                hidden = ring_gather(hidden, "ra", PAIR, groups, g)
                outs_own = outs_own + dot(hidden, d_own)
                outs_other = outs_other + dot(hidden, d_other)
            gate_open = tuple(h[:1] for h in opened)
            out = jnp.concatenate((outs_own, outs_other), axis=1)
            out = part(out, core, chunk // 2) + swap(part(out, 1 - core, chunk // 2).astype(BF16), "cb").astype(F32)
            rows = chunk // cb
            out = ring_reduce(lambda at: part(out, at, rows), "cb", 2, rows_y, y)
            branch = out[:, :width] + swap(out[:, width:].astype(BF16), "ra").astype(F32)
            mine = lax.dynamic_slice_in_dim(own, core * (chunk // 2) + y * rows, rows, 0)
            mixed = RESIDUAL * mine.astype(F32) + branch
            stats = sum_over_ra(jnp.stack((jnp.sum(mixed, axis=1), jnp.sum(mixed * mixed, axis=1))))
            mean = stats[0] / full_width
            var = stats[1] / full_width - mean * mean
            normed = (mixed - mean[:, None]) * lax.rsqrt(var + EPSILON)[:, None]
            normed = (normed * norm_gain[layer] + norm_shift[layer]).astype(BF16)
            if not last:
                normed = jnp.concatenate((normed, swap(normed, "ra")), axis=1)
            whole = swap_gather(ring_gather(normed, "cb", 2, rows_y, y), "cb", core)
            after.append(whole if last else (whole[:, :width], whole[:, width:]))
        streams = after
    return jnp.concatenate(streams, axis=0)


def solution(mesh):
    return jax.shard_map(
        per_device,
        mesh=mesh,
        in_specs=(
            P(None, "ra"),
            P(None, "ra", "cb"),
            P(None, "ra", "cb"),
            P(None, "cb", "ra"),
            P(None, "ra"),
            P(None, "ra"),
        ),
        out_specs=P(None, "ra"),
        check_vma=False,
    )
```

profile of v0, /device:TPU:0, one launch (start us, length us, event | category | flops | bytes accessed | tf_op | source)
XLA Modules:
  0.0 642.9 jit_solution(13288860886107505483)
XLA Ops:
  0.0 4.7 dynamic-slice_bitcast_fusion.3
  28.0 4.9 dynamic-slice_bitcast_fusion.11
  51.9 3.9 collective-permute-done.51
  79.1 8.1 %collective-permute-done.3 = bf16[128,1536]{1,0:T(8,128)(2,1)S(1)} collective-permute-done((bf16[128,1536]{1,0:T(8,128)(2,1)S(1)}, bf16[128,1536]{1,0:T(8,128)(2,1)S(1)}, u32[]{:S(2)}, u32[]{:S(2)}) %collective-permute-start.3) | collective-permute-done | bytes 393248 | tf_op jit(solution)/shard_map/ppermute | solution.py:44
  87.7 7.9 %collective-permute-done.53 = bf16[128,1536]{1,0:T(8,128)(2,1)S(1)} collective-permute-done((bf16[128,1536]{1,0:T(8,128)(2,1)S(1)}, bf16[128,1536]{1,0:T(8,128)(2,1)S(1)}, u32[]{:S(2)}, u32[]{:S(2)}) %collective-permute-start.53) | collective-permute-done | bytes 393248 | tf_op jit(solution)/shard_map/ppermute | solution.py:44
  96.4 7.7 %collective-permute-done.96 = bf16[128,1536]{1,0:T(8,128)(2,1)S(1)} collective-permute-done((bf16[128,1536]{1,0:T(8,128)(2,1)S(1)}, bf16[128,1536]{1,0:T(8,128)(2,1)S(1)}, u32[]{:S(2)}, u32[]{:S(2)}) %collective-permute-start.96) | collective-permute-done | bytes 393248 | tf_op jit(solution)/shard_map/ppermute | solution.py:44
  104.6 7.9 %collective-permute-done.4 = bf16[128,1536]{1,0:T(8,128)(2,1)S(1)} collective-permute-done((bf16[128,1536]{1,0:T(8,128)(2,1)S(1)}, bf16[128,1536]{1,0:T(8,128)(2,1)S(1)}, u32[]{:S(2)}, u32[]{:S(2)}) %collective-permute-start.4) | collective-permute-done | bytes 393248 | tf_op jit(solution)/shard_map/ppermute | solution.py:44
  113.0 7.9 %collective-permute-done.54 = bf16[128,1536]{1,0:T(8,128)(2,1)S(1)} collective-permute-done((bf16[128,1536]{1,0:T(8,128)(2,1)S(1)}, bf16[128,1536]{1,0:T(8,128)(2,1)S(1)}, u32[]{:S(2)}, u32[]{:S(2)}) %collective-permute-start.54) | collective-permute-done | bytes 393248 | tf_op jit(solution)/shard_map/ppermute | solution.py:44
  121.4 7.9 %collective-permute-done.97 = bf16[128,1536]{1,0:T(8,128)(2,1)S(1)} collective-permute-done((bf16[128,1536]{1,0:T(8,128)(2,1)S(1)}, bf16[128,1536]{1,0:T(8,128)(2,1)S(1)}, u32[]{:S(2)}, u32[]{:S(2)}) %collective-permute-start.97) | collective-permute-done | bytes 393248 | tf_op jit(solution)/shard_map/ppermute | solution.py:44
  129.8 7.9 %collective-permute-done.5 = bf16[128,1536]{1,0:T(8,128)(2,1)S(1)} collective-permute-done((bf16[128,1536]{1,0:T(8,128)(2,1)S(1)}, bf16[128,1536]{1,0:T(8,128)(2,1)S(1)}, u32[]{:S(2)}, u32[]{:S(2)}) %collective-permute-start.5) | collective-permute-done | bytes 393248 | tf_op jit(solution)/shard_map/ppermute | solution.py:44
  138.5 7.7 %collective-permute-done.55 = bf16[128,1536]{1,0:T(8,128)(2,1)S(1)} collective-permute-done((bf16[128,1536]{1,0:T(8,128)(2,1)S(1)}, bf16[128,1536]{1,0:T(8,128)(2,1)S(1)}, u32[]{:S(2)}, u32[]{:S(2)}) %collective-permute-start.55) | collective-permute-done | bytes 393248 | tf_op jit(solution)/shard_map/ppermute | solution.py:44
  146.9 7.8 %collective-permute-done.98 = bf16[128,1536]{1,0:T(8,128)(2,1)S(1)} collective-permute-done((bf16[128,1536]{1,0:T(8,128)(2,1)S(1)}, bf16[128,1536]{1,0:T(8,128)(2,1)S(1)}, u32[]{:S(2)}, u32[]{:S(2)}) %collective-permute-start.98) | collective-permute-done | bytes 393248 | tf_op jit(solution)/shard_map/ppermute | solution.py:44
  163.1 4.2 collective-permute-done.99
  167.3 18.2 %collective-permute-done.7 = bf16[128,768]{1,0:T(8,128)(2,1)S(1)} collective-permute-done((bf16[128,768]{1,0:T(8,128)(2,1)S(1)}, bf16[128,768]{1,0:T(8,128)(2,1)S(1)}, u32[]{:S(2)}, u32[]{:S(2)}) %collective-permute-start.7) | collective-permute-done | bytes 196640 | tf_op jit(solution)/shard_map/ppermute | solution.py:55
  185.6 3.9 collective-permute-done.57
  189.5 4.1 collective-permute-done.100
  197.8 4.0 collective-permute-done.102
  202.2 3.8 collective-permute-done.8
  206.1 4.2 collective-permute-done.58
  210.3 4.2 collective-permute-done.101
  214.5 7.0 %collective-permute-done.11 = bf16[128,1280]{1,0:T(8,128)(2,1)S(1)} collective-permute-done((bf16[128,1280]{1,0:T(8,128)(2,1)S(1)}, bf16[128,1280]{1,0:T(8,128)(2,1)S(1)}, u32[]{:S(2)}, u32[]{:S(2)}) %collective-permute-start.11) | collective-permute-done | bytes 327712 | tf_op jit(solution)/shard_map/ppermute | solution.py:44
  222.0 6.6 %collective-permute-done.60 = bf16[128,1280]{1,0:T(8,128)(2,1)S(1)} collective-permute-done((bf16[128,1280]{1,0:T(8,128)(2,1)S(1)}, bf16[128,1280]{1,0:T(8,128)(2,1)S(1)}, u32[]{:S(2)}, u32[]{:S(2)}) %collective-permute-start.60) | collective-permute-done | bytes 327712 | tf_op jit(solution)/shard_map/ppermute | solution.py:44
  229.0 6.5 %collective-permute-done.103 = bf16[128,1280]{1,0:T(8,128)(2,1)S(1)} collective-permute-done((bf16[128,1280]{1,0:T(8,128)(2,1)S(1)}, bf16[128,1280]{1,0:T(8,128)(2,1)S(1)}, u32[]{:S(2)}, u32[]{:S(2)}) %collective-permute-start.103) | collective-permute-done | bytes 327712 | tf_op jit(solution)/shard_map/ppermute | solution.py:44
  236.4 6.2 collective-permute-done.12
  243.2 6.4 collective-permute-done.61
  250.2 6.4 collective-permute-done.104
  263.7 3.5 collective-permute-done.105
  295.0 5.1 collective-permute-done.19
  300.5 5.2 collective-permute-done.66
  306.2 4.2 collective-permute-done.109
  310.9 6.8 %collective-permute-done.20 = bf16[128,512]{0,1:T(8,128)(2,1)S(1)} collective-permute-done((bf16[128,512]{0,1:T(8,128)(2,1)S(1)}, bf16[128,512]{0,1:T(8,128)(2,1)S(1)}, u32[]{:S(2)}, u32[]{:S(2)}) %collective-permute-start.20) | collective-permute-done | bytes 131104 | tf_op jit(solution)/shard_map/ppermute | solution.py:33
  335.2 5.0 collective-permute-done.114
  349.1 4.8 collective-permute-done.72
  354.1 4.0 collective-permute-done.25
  376.4 8.1 %collective-permute-done.117 = bf16[128,1536]{1,0:T(8,128)(2,1)S(1)} collective-permute-done((bf16[128,1536]{1,0:T(8,128)(2,1)S(1)}, bf16[128,1536]{1,0:T(8,128)(2,1)S(1)}, u32[]{:S(2)}, u32[]{:S(2)}) %collective-permute-start.117) | collective-permute-done | bytes 393248 | tf_op jit(solution)/shard_map/ppermute | solution.py:44
  385.0 7.9 %collective-permute-done.74 = bf16[128,1536]{1,0:T(8,128)(2,1)S(1)} collective-permute-done((bf16[128,1536]{1,0:T(8,128)(2,1)S(1)}, bf16[128,1536]{1,0:T(8,128)(2,1)S(1)}, u32[]{:S(2)}, u32[]{:S(2)}) %collective-permute-start.74) | collective-permute-done | bytes 393248 | tf_op jit(solution)/shard_map/ppermute | solution.py:44
  393.4 7.9 %collective-permute-done.28 = bf16[128,1536]{1,0:T(8,128)(2,1)S(1)} collective-permute-done((bf16[128,1536]{1,0:T(8,128)(2,1)S(1)}, bf16[128,1536]{1,0:T(8,128)(2,1)S(1)}, u32[]{:S(2)}, u32[]{:S(2)}) %collective-permute-start.28) | collective-permute-done | bytes 393248 | tf_op jit(solution)/shard_map/ppermute | solution.py:44
  401.9 7.9 %collective-permute-done.118 = bf16[128,1536]{1,0:T(8,128)(2,1)S(1)} collective-permute-done((bf16[128,1536]{1,0:T(8,128)(2,1)S(1)}, bf16[128,1536]{1,0:T(8,128)(2,1)S(1)}, u32[]{:S(2)}, u32[]{:S(2)}) %collective-permute-start.118) | collective-permute-done | bytes 393248 | tf_op jit(solution)/shard_map/ppermute | solution.py:44
  410.3 7.9 %collective-permute-done.75 = bf16[128,1536]{1,0:T(8,128)(2,1)S(1)} collective-permute-done((bf16[128,1536]{1,0:T(8,128)(2,1)S(1)}, bf16[128,1536]{1,0:T(8,128)(2,1)S(1)}, u32[]{:S(2)}, u32[]{:S(2)}) %collective-permute-start.75) | collective-permute-done | bytes 393248 | tf_op jit(solution)/shard_map/ppermute | solution.py:44
  418.7 7.9 %collective-permute-done.29 = bf16[128,1536]{1,0:T(8,128)(2,1)S(1)} collective-permute-done((bf16[128,1536]{1,0:T(8,128)(2,1)S(1)}, bf16[128,1536]{1,0:T(8,128)(2,1)S(1)}, u32[]{:S(2)}, u32[]{:S(2)}) %collective-permute-start.29) | collective-permute-done | bytes 393248 | tf_op jit(solution)/shard_map/ppermute | solution.py:44
  430.0 5.1 collective-permute-done.119
  435.7 7.8 %collective-permute-done.76 = bf16[128,1536]{1,0:T(8,128)(2,1)S(1)} collective-permute-done((bf16[128,1536]{1,0:T(8,128)(2,1)S(1)}, bf16[128,1536]{1,0:T(8,128)(2,1)S(1)}, u32[]{:S(2)}, u32[]{:S(2)}) %collective-permute-start.76) | collective-permute-done | bytes 393248 | tf_op jit(solution)/shard_map/ppermute | solution.py:44
  443.9 8.0 %collective-permute-done.30 = bf16[128,1536]{1,0:T(8,128)(2,1)S(1)} collective-permute-done((bf16[128,1536]{1,0:T(8,128)(2,1)S(1)}, bf16[128,1536]{1,0:T(8,128)(2,1)S(1)}, u32[]{:S(2)}, u32[]{:S(2)}) %collective-permute-start.30) | collective-permute-done | bytes 393248 | tf_op jit(solution)/shard_map/ppermute | solution.py:44
  452.7 6.2 collective-permute-done.123
  459.3 6.6 %collective-permute-done.80 = bf16[128,1280]{1,0:T(8,128)(2,1)S(1)} collective-permute-done((bf16[128,1280]{1,0:T(8,128)(2,1)S(1)}, bf16[128,1280]{1,0:T(8,128)(2,1)S(1)}, u32[]{:S(2)}, u32[]{:S(2)}) %collective-permute-start.80) | collective-permute-done | bytes 327712 | tf_op jit(solution)/shard_map/ppermute | solution.py:44
  466.4 6.6 %collective-permute-done.35 = bf16[128,1280]{1,0:T(8,128)(2,1)S(1)} collective-permute-done((bf16[128,1280]{1,0:T(8,128)(2,1)S(1)}, bf16[128,1280]{1,0:T(8,128)(2,1)S(1)}, u32[]{:S(2)}, u32[]{:S(2)}) %collective-permute-start.35) | collective-permute-done | bytes 327712 | tf_op jit(solution)/shard_map/ppermute | solution.py:44
  473.4 3.8 collective-permute-done.120
  477.3 4.2 collective-permute-done.77
  481.5 4.2 collective-permute-done.31
  485.7 18.2 %collective-permute-done.121 = bf16[128,768]{1,0:T(8,128)(2,1)S(1)} collective-permute-done((bf16[128,768]{1,0:T(8,128)(2,1)S(1)}, bf16[128,768]{1,0:T(8,128)(2,1)S(1)}, u32[]{:S(2)}, u32[]{:S(2)}) %collective-permute-start.121) | collective-permute-done | bytes 196640 | tf_op jit(solution)/shard_map/ppermute | solution.py:55
  503.9 3.9 collective-permute-done.78
  507.9 4.2 collective-permute-done.32
  515.0 5.2 collective-permute-done.36
  520.6 3.8 collective-permute-done.122
  524.5 4.2 collective-permute-done.79
  528.7 4.2 collective-permute-done.33
  534.0 5.9 collective-permute-done.125
  540.5 6.4 collective-permute-done.82
  547.5 6.4 collective-permute-done.37
  592.3 5.1 collective-permute-done.130
  598.6 4.4 collective-permute-done.87
  604.2 3.5 collective-permute-done.44
  628.1 4.5 collective-permute-done.49
  634.4 4.5 collective-permute-done.92
  (598 shorter events, 246.5 us)
Async XLA Ops:
  6.0 65.1 %collective-permute-start.2 = (bf16[512,1536]{1,0:T(8,128)(2,1)}, bf16[512,1536]{1,0:T(8,128)(2,1)S(1)}, u32[]{:S(2)}, u32[]{:S(2)}) collective-permute-start(bf16[512,1536]{1,0:T(8,128)(2,1)} %pad_maximum_fusion.1), channel_id=1, source_target_pairs={{0,4},{4,0},{8,12},{12,8},{16,20},{20,16},{24,28},{28,24},{1,5},{5... | collective-permute-start | bytes 4718600 | tf_op jit(solution)/shard_map/ppermute | solution.py:33
  13.4 43.7 %collective-permute-start = (bf16[256,512]{0,1:T(8,128)(2,1)}, bf16[256,512]{0,1:T(8,128)(2,1)}, u32[]{:S(2)}, u32[]{:S(2)}) collective-permute-start(bf16[256,512]{0,1:T(8,128)(2,1)} %copy.14), channel_id=1, source_target_pairs={{0,4},{4,0},{8,12},{12,8},{16,20},{20,16},{24,28},{28,24},{1,5},{5... | collective-permute-start | bytes 786440 | tf_op jit(solution)/shard_map/ppermute | solution.py:33
  17.1 38.7 %collective-permute-start.51 = (bf16[256,512]{0,1:T(8,128)(2,1)}, bf16[256,512]{0,1:T(8,128)(2,1)}, u32[]{:S(2)}, u32[]{:S(2)}) collective-permute-start(bf16[256,512]{0,1:T(8,128)(2,1)} %constant_dynamic-slice_fusion.1), channel_id=1, source_target_pairs={{0,4},{4,0},{8,12},{12,8},{16,20},{20,16},{24,28},{28,24},{1,5},{5... | collective-permute-start | bytes 786440 | tf_op jit(solution)/shard_map/ppermute | solution.py:33
  22.8 37.7 %collective-permute-start.94 = (bf16[256,512]{0,1:T(8,128)(2,1)}, bf16[256,512]{0,1:T(8,128)(2,1)}, u32[]{:S(2)}, u32[]{:S(2)}) collective-permute-start(bf16[256,512]{0,1:T(8,128)(2,1)} %constant_dynamic-slice_fusion), channel_id=1, source_target_pairs={{0,4},{4,0},{8,12},{12,8},{16,20},{20,16},{24,28},{28,24},{1,5},{5... | collective-permute-start | bytes 786440 | tf_op jit(solution)/shard_map/ppermute | solution.py:33
  71.1 84.2 %collective-permute-start.9 = (bf16[512,1280]{1,0:T(8,128)(2,1)S(1)}, bf16[512,1280]{1,0:T(8,128)(2,1)S(1)}, u32[]{:S(2)}, u32[]{:S(2)}) collective-permute-start(bf16[512,1280]{1,0:T(8,128)(2,1)S(1)} %pad_maximum_fusion.5), channel_id=1, source_target_pairs={{0,4},{4,0},{8,12},{12,8},{16,20},{20,16},{24,28},{28,24},{1,5},{5... | collective-permute-start | bytes 3932168 | tf_op jit(solution)/shard_map/ppermute | solution.py:33
  73.4 13.8 %collective-permute-start.3 = (bf16[128,1536]{1,0:T(8,128)(2,1)S(1)}, bf16[128,1536]{1,0:T(8,128)(2,1)S(1)}, u32[]{:S(2)}, u32[]{:S(2)}) collective-permute-start(bf16[128,1536]{1,0:T(8,128)(2,1)S(1)} %fusion), channel_id=1, source_target_pairs={{0,8},{4,12},{8,16},{12,20},{16,24},{20,28},{24,0},{28,4},{1,9},{5... | collective-permute-start | bytes 1179656 | tf_op jit(solution)/shard_map/ppermute | solution.py:44
  75.4 20.2 %collective-permute-start.53 = (bf16[128,1536]{1,0:T(8,128)(2,1)S(1)}, bf16[128,1536]{1,0:T(8,128)(2,1)S(1)}, u32[]{:S(2)}, u32[]{:S(2)}) collective-permute-start(bf16[128,1536]{1,0:T(8,128)(2,1)S(1)} %fusion.2), channel_id=1, source_target_pairs={{0,8},{4,12},{8,16},{12,20},{16,24},{20,28},{24,0},{28,4},{1,9},{5... | collective-permute-start | bytes 1179656 | tf_op jit(solution)/shard_map/ppermute | solution.py:44
  77.5 26.6 %collective-permute-start.96 = (bf16[128,1536]{1,0:T(8,128)(2,1)S(1)}, bf16[128,1536]{1,0:T(8,128)(2,1)S(1)}, u32[]{:S(2)}, u32[]{:S(2)}) collective-permute-start(bf16[128,1536]{1,0:T(8,128)(2,1)S(1)} %fusion.4), channel_id=1, source_target_pairs={{0,8},{4,12},{8,16},{12,20},{16,24},{20,28},{24,0},{28,4},{1,9},{5... | collective-permute-start | bytes 1179656 | tf_op jit(solution)/shard_map/ppermute | solution.py:44
  87.7 24.8 %collective-permute-start.4 = (bf16[128,1536]{1,0:T(8,128)(2,1)S(1)}, bf16[128,1536]{1,0:T(8,128)(2,1)S(1)}, u32[]{:S(2)}, u32[]{:S(2)}) collective-permute-start(bf16[128,1536]{1,0:T(8,128)(2,1)S(1)} %add_convert_fusion.11), channel_id=1, source_target_pairs={{0,8},{4,12},{8,16},{12,20},{16,24},{20,28},{24,0},{28,4},{1,9},{5... | collective-permute-start | bytes 1179656 | tf_op jit(solution)/shard_map/ppermute | solution.py:44
  96.1 24.9 %collective-permute-start.54 = (bf16[128,1536]{1,0:T(8,128)(2,1)S(1)}, bf16[128,1536]{1,0:T(8,128)(2,1)S(1)}, u32[]{:S(2)}, u32[]{:S(2)}) collective-permute-start(bf16[128,1536]{1,0:T(8,128)(2,1)S(1)} %add_convert_fusion.7), channel_id=1, source_target_pairs={{0,8},{4,12},{8,16},{12,20},{16,24},{20,28},{24,0},{28,4},{1,9},{5... | collective-permute-start | bytes 1179656 | tf_op jit(solution)/shard_map/ppermute | solution.py:44
  104.5 24.9 %collective-permute-start.97 = (bf16[128,1536]{1,0:T(8,128)(2,1)S(1)}, bf16[128,1536]{1,0:T(8,128)(2,1)S(1)}, u32[]{:S(2)}, u32[]{:S(2)}) collective-permute-start(bf16[128,1536]{1,0:T(8,128)(2,1)S(1)} %add_convert_fusion.3), channel_id=1, source_target_pairs={{0,8},{4,12},{8,16},{12,20},{16,24},{20,28},{24,0},{28,4},{1,9},{5... | collective-permute-start | bytes 1179656 | tf_op jit(solution)/shard_map/ppermute | solution.py:44
  112.9 24.8 %collective-permute-start.5 = (bf16[128,1536]{1,0:T(8,128)(2,1)S(1)}, bf16[128,1536]{1,0:T(8,128)(2,1)S(1)}, u32[]{:S(2)}, u32[]{:S(2)}) collective-permute-start(bf16[128,1536]{1,0:T(8,128)(2,1)S(1)} %add_convert_fusion.10), channel_id=1, source_target_pairs={{0,8},{4,12},{8,16},{12,20},{16,24},{20,28},{24,0},{28,4},{1,9},{5... | collective-permute-start | bytes 1179656 | tf_op jit(solution)/shard_map/ppermute | solution.py:44
  121.3 24.9 %collective-permute-start.55 = (bf16[128,1536]{1,0:T(8,128)(2,1)S(1)}, bf16[128,1536]{1,0:T(8,128)(2,1)S(1)}, u32[]{:S(2)}, u32[]{:S(2)}) collective-permute-start(bf16[128,1536]{1,0:T(8,128)(2,1)S(1)} %add_convert_fusion.6), channel_id=1, source_target_pairs={{0,8},{4,12},{8,16},{12,20},{16,24},{20,28},{24,0},{28,4},{1,9},{5... | collective-permute-start | bytes 1179656 | tf_op jit(solution)/shard_map/ppermute | solution.py:44
  129.8 24.9 %collective-permute-start.98 = (bf16[128,1536]{1,0:T(8,128)(2,1)S(1)}, bf16[128,1536]{1,0:T(8,128)(2,1)S(1)}, u32[]{:S(2)}, u32[]{:S(2)}) collective-permute-start(bf16[128,1536]{1,0:T(8,128)(2,1)S(1)} %add_convert_fusion.2), channel_id=1, source_target_pairs={{0,8},{4,12},{8,16},{12,20},{16,24},{20,28},{24,0},{28,4},{1,9},{5... | collective-permute-start | bytes 1179656 | tf_op jit(solution)/shard_map/ppermute | solution.py:44
  138.4 20.4 %collective-permute-start.6 = (bf16[128,768]{1,0:T(8,128)(2,1)S(1)}, bf16[128,768]{1,0:T(8,128)(2,1)S(1)}, u32[]{:S(2)}, u32[]{:S(2)}) collective-permute-start(bf16[128,768]{1,0:T(8,128)(2,1)S(1)} %get-tuple-element.83), channel_id=1, source_target_pairs={{0,8},{4,12},{8,16},{12,20},{16,24},{20,28},{24,0},{28,4},{1,9},{5... | collective-permute-start | bytes 589832 | tf_op jit(solution)/shard_map/ppermute | solution.py:55
  146.8 16.2 %collective-permute-start.56 = (bf16[128,768]{1,0:T(8,128)(2,1)S(1)}, bf16[128,768]{1,0:T(8,128)(2,1)S(1)}, u32[]{:S(2)}, u32[]{:S(2)}) collective-permute-start(bf16[128,768]{1,0:T(8,128)(2,1)S(1)} %get-tuple-element.72), channel_id=1, source_target_pairs={{0,8},{4,12},{8,16},{12,20},{16,24},{20,28},{24,0},{28,4},{1,9},{5... | collective-permute-start | bytes 589832 | tf_op jit(solution)/shard_map/ppermute | solution.py:55
  156.5 37.2 %collective-permute-start.10 = (bf16[128,1280]{1,0:T(8,128)(2,1)S(1)}, bf16[128,1280]{1,0:T(8,128)(2,1)S(1)}, u32[]{:S(2)}, u32[]{:S(2)}) collective-permute-start(bf16[128,1280]{1,0:T(8,128)(2,1)S(1)} %fusion.6), channel_id=1, source_target_pairs={{0,8},{4,12},{8,16},{12,20},{16,24},{20,28},{24,0},{28,4},{1,9},{5... | collective-permute-start | bytes 983048 | tf_op jit(solution)/shard_map/ppermute | solution.py:44
  157.1 78.9 %collective-permute-start.16 = (bf16[768,512]{1,0:T(8,128)(2,1)S(1)}, bf16[768,512]{1,0:T(8,128)(2,1)S(1)}, u32[]{:S(2)}, u32[]{:S(2)}) collective-permute-start(bf16[768,512]{1,0:T(8,128)(2,1)S(1)} %copy-done.18), channel_id=1, source_target_pairs={{0,4},{4,0},{8,12},{12,8},{16,20},{20,16},{24,28},{28,24},{1,5},{5... | collective-permute-start | bytes 2359304 | tf_op jit(solution)/shard_map/ppermute | solution.py:33
  158.8 36.9 %collective-permute-start.59 = (bf16[128,1280]{1,0:T(8,128)(2,1)S(1)}, bf16[128,1280]{1,0:T(8,128)(2,1)S(1)}, u32[]{:S(2)}, u32[]{:S(2)}) collective-permute-start(bf16[128,1280]{1,0:T(8,128)(2,1)S(1)} %fusion.8), channel_id=1, source_target_pairs={{0,8},{4,12},{8,16},{12,20},{16,24},{20,28},{24,0},{28,4},{1,9},{5... | collective-permute-start | bytes 983048 | tf_op jit(solution)/shard_map/ppermute | solution.py:44
  163.1 22.5 %collective-permute-start.7 = (bf16[128,768]{1,0:T(8,128)(2,1)S(1)}, bf16[128,768]{1,0:T(8,128)(2,1)S(1)}, u32[]{:S(2)}, u32[]{:S(2)}) collective-permute-start(bf16[128,768]{1,0:T(8,128)(2,1)S(1)} %collective-permute-done.6), channel_id=1, source_target_pairs={{0,8},{4,12},{8,16},{12,20},{16,24},{20,28},{24,0},{28,4},{1,9},{5... | collective-permute-start | bytes 589832 | tf_op jit(solution)/shard_map/ppermute | solution.py:55
  167.3 22.2 %collective-permute-start.57 = (bf16[128,768]{1,0:T(8,128)(2,1)S(1)}, bf16[128,768]{1,0:T(8,128)(2,1)S(1)}, u32[]{:S(2)}, u32[]{:S(2)}) collective-permute-start(bf16[128,768]{1,0:T(8,128)(2,1)S(1)} %collective-permute-done.56), channel_id=1, source_target_pairs={{0,8},{4,12},{8,16},{12,20},{16,24},{20,28},{24,0},{28,4},{1,9},{5... | collective-permute-start | bytes 589832 | tf_op jit(solution)/shard_map/ppermute | solution.py:55
  193.7 16.5 %collective-permute-start.58 = (bf16[128,768]{1,0:T(8,128)(2,1)S(1)}, bf16[128,768]{1,0:T(8,128)(2,1)S(1)}, u32[]{:S(2)}, u32[]{:S(2)}) collective-permute-start(bf16[128,768]{1,0:T(8,128)(2,1)S(1)} %collective-permute-done.57), channel_id=1, source_target_pairs={{0,8},{4,12},{8,16},{12,20},{16,24},{20,28},{24,0},{28,4},{1,9},{5... | collective-permute-start | bytes 589832 | tf_op jit(solution)/shard_map/ppermute | solution.py:55
  195.8 18.7 %collective-permute-start.101 = (bf16[128,768]{1,0:T(8,128)(2,1)S(1)}, bf16[128,768]{1,0:T(8,128)(2,1)S(1)}, u32[]{:S(2)}, u32[]{:S(2)}) collective-permute-start(bf16[128,768]{1,0:T(8,128)(2,1)S(1)} %collective-permute-done.100), channel_id=1, source_target_pairs={{0,8},{4,12},{8,16},{12,20},{16,24},{20,28},{24,0},{28,4},{1,9},{5... | collective-permute-start | bytes 589832 | tf_op jit(solution)/shard_map/ppermute | solution.py:55
  201.8 19.7 %collective-permute-start.11 = (bf16[128,1280]{1,0:T(8,128)(2,1)S(1)}, bf16[128,1280]{1,0:T(8,128)(2,1)S(1)}, u32[]{:S(2)}, u32[]{:S(2)}) collective-permute-start(bf16[128,1280]{1,0:T(8,128)(2,1)S(1)} %add_convert_fusion.23), channel_id=1, source_target_pairs={{0,8},{4,12},{8,16},{12,20},{16,24},{20,28},{24,0},{28,4},{1,9},{5... | collective-permute-start | bytes 983048 | tf_op jit(solution)/shard_map/ppermute | solution.py:44
  206.0 22.5 %collective-permute-start.60 = (bf16[128,1280]{1,0:T(8,128)(2,1)S(1)}, bf16[128,1280]{1,0:T(8,128)(2,1)S(1)}, u32[]{:S(2)}, u32[]{:S(2)}) collective-permute-start(bf16[128,1280]{1,0:T(8,128)(2,1)S(1)} %add_convert_fusion.19), channel_id=1, source_target_pairs={{0,8},{4,12},{8,16},{12,20},{16,24},{20,28},{24,0},{28,4},{1,9},{5... | collective-permute-start | bytes 983048 | tf_op jit(solution)/shard_map/ppermute | solution.py:44
  210.3 25.3 %collective-permute-start.103 = (bf16[128,1280]{1,0:T(8,128)(2,1)S(1)}, bf16[128,1280]{1,0:T(8,128)(2,1)S(1)}, u32[]{:S(2)}, u32[]{:S(2)}) collective-permute-start(bf16[128,1280]{1,0:T(8,128)(2,1)S(1)} %add_convert_fusion.15), channel_id=1, source_target_pairs={{0,8},{4,12},{8,16},{12,20},{16,24},{20,28},{24,0},{28,4},{1,9},{5... | collective-permute-start | bytes 983048 | tf_op jit(solution)/shard_map/ppermute | solution.py:44
  221.9 20.7 %collective-permute-start.12 = (bf16[128,1280]{1,0:T(8,128)(2,1)S(1)}, bf16[128,1280]{1,0:T(8,128)(2,1)S(1)}, u32[]{:S(2)}, u32[]{:S(2)}) collective-permute-start(bf16[128,1280]{1,0:T(8,128)(2,1)S(1)} %add_convert_fusion.22), channel_id=1, source_target_pairs={{0,8},{4,12},{8,16},{12,20},{16,24},{20,28},{24,0},{28,4},{1,9},{5... | collective-permute-start | bytes 983048 | tf_op jit(solution)/shard_map/ppermute | solution.py:44
  228.9 20.7 %collective-permute-start.61 = (bf16[128,1280]{1,0:T(8,128)(2,1)S(1)}, bf16[128,1280]{1,0:T(8,128)(2,1)S(1)}, u32[]{:S(2)}, u32[]{:S(2)}) collective-permute-start(bf16[128,1280]{1,0:T(8,128)(2,1)S(1)} %add_convert_fusion.18), channel_id=1, source_target_pairs={{0,8},{4,12},{8,16},{12,20},{16,24},{20,28},{24,0},{28,4},{1,9},{5... | collective-permute-start | bytes 983048 | tf_op jit(solution)/shard_map/ppermute | solution.py:44
  235.9 20.7 %collective-permute-start.104 = (bf16[128,1280]{1,0:T(8,128)(2,1)S(1)}, bf16[128,1280]{1,0:T(8,128)(2,1)S(1)}, u32[]{:S(2)}, u32[]{:S(2)}) collective-permute-start(bf16[128,1280]{1,0:T(8,128)(2,1)S(1)} %add_convert_fusion.14), channel_id=1, source_target_pairs={{0,8},{4,12},{8,16},{12,20},{16,24},{20,28},{24,0},{28,4},{1,9},{5... | collective-permute-start | bytes 983048 | tf_op jit(solution)/shard_map/ppermute | solution.py:44
  236.0 42.2 %collective-permute-start.17 = (bf16[640,512]{1,0:T(8,128)(2,1)S(1)}, bf16[640,512]{1,0:T(8,128)(2,1)S(1)}, u32[]{:S(2)}, u32[]{:S(2)}) collective-permute-start(bf16[640,512]{1,0:T(8,128)(2,1)S(1)} %copy-done.22), channel_id=1, source_target_pairs={{0,4},{4,0},{8,12},{12,8},{16,20},{20,16},{24,28},{28,24},{1,5},{5... | collective-permute-start | bytes 1966088 | tf_op jit(solution)/shard_map/ppermute | solution.py:33
  243.1 17.0 %collective-permute-start.13 = (bf16[128,640]{1,0:T(8,128)(2,1)S(1)}, bf16[128,640]{1,0:T(8,128)(2,1)S(1)}, u32[]{:S(2)}, u32[]{:S(2)}) collective-permute-start(bf16[128,640]{1,0:T(8,128)(2,1)S(1)} %get-tuple-element.85), channel_id=1, source_target_pairs={{0,8},{4,12},{8,16},{12,20},{16,24},{20,28},{24,0},{28,4},{1,9},{5... | collective-permute-start | bytes 491528 | tf_op jit(solution)/shard_map/ppermute | solution.py:55
  278.2 80.0 %collective-permute-start.27 = (bf16[512,1536]{1,0:T(8,128)(2,1)}, bf16[512,1536]{1,0:T(8,128)(2,1)S(1)}, u32[]{:S(2)}, u32[]{:S(2)}) collective-permute-start(bf16[512,1536]{1,0:T(8,128)(2,1)} %pad_maximum_fusion.3), channel_id=1, source_target_pairs={{0,4},{4,0},{8,12},{12,8},{16,20},{20,16},{24,28},{28,24},{1,5},{5... | collective-permute-start | bytes 4718600 | tf_op jit(solution)/shard_map/ppermute | solution.py:33
  293.4 16.9 %collective-permute-start.109 = (bf16[128,1024]{0,1:T(8,128)(2,1)S(1)}, bf16[128,1024]{0,1:T(8,128)(2,1)S(1)}, u32[]{:S(2)}, u32[]{:S(2)}) collective-permute-start(bf16[128,1024]{0,1:T(8,128)(2,1)S(1)} %dynamic-slice_convert_fusion.1), channel_id=1, source_target_pairs={{0,2},{1,3},{2,0},{3,1},{4,6},{5,7},{6,4},{7,5},{8,10},{9,11},{10,... | collective-permute-start | bytes 786440 | tf_op jit(solution)/shard_map/ppermute | solution.py:44
  300.2 17.5 %collective-permute-start.20 = (bf16[128,512]{0,1:T(8,128)(2,1)S(1)}, bf16[128,512]{0,1:T(8,128)(2,1)S(1)}, u32[]{:S(2)}, u32[]{:S(2)}) collective-permute-start(bf16[128,512]{0,1:T(8,128)(2,1)S(1)} %slice.435), channel_id=1, source_target_pairs={{0,4},{4,0},{8,12},{12,8},{16,20},{20,16},{24,28},{28,24},{1,5},{5... | collective-permute-start | bytes 393224 | tf_op jit(solution)/shard_map/ppermute | solution.py:33
  358.2 68.9 %collective-permute-start.34 = (bf16[512,1280]{1,0:T(8,128)(2,1)S(1)}, bf16[512,1280]{1,0:T(8,128)(2,1)S(1)}, u32[]{:S(2)}, u32[]{:S(2)}) collective-permute-start(bf16[512,1280]{1,0:T(8,128)(2,1)S(1)} %pad_maximum_fusion.7), channel_id=1, source_target_pairs={{0,4},{4,0},{8,12},{12,8},{16,20},{20,16},{24,28},{28,24},{1,5},{5... | collective-permute-start | bytes 3932168 | tf_op jit(solution)/shard_map/ppermute | solution.py:33
  370.7 13.8 %collective-permute-start.117 = (bf16[128,1536]{1,0:T(8,128)(2,1)S(1)}, bf16[128,1536]{1,0:T(8,128)(2,1)S(1)}, u32[]{:S(2)}, u32[]{:S(2)}) collective-permute-start(bf16[128,1536]{1,0:T(8,128)(2,1)S(1)} %fusion.5), channel_id=1, source_target_pairs={{0,8},{4,12},{8,16},{12,20},{16,24},{20,28},{24,0},{28,4},{1,9},{5... | collective-permute-start | bytes 1179656 | tf_op jit(solution)/shard_map/ppermute | solution.py:44
  372.3 20.7 %collective-permute-start.74 = (bf16[128,1536]{1,0:T(8,128)(2,1)S(1)}, bf16[128,1536]{1,0:T(8,128)(2,1)S(1)}, u32[]{:S(2)}, u32[]{:S(2)}) collective-permute-start(bf16[128,1536]{1,0:T(8,128)(2,1)S(1)} %fusion.3), channel_id=1, source_target_pairs={{0,8},{4,12},{8,16},{12,20},{16,24},{20,28},{24,0},{28,4},{1,9},{5... | collective-permute-start | bytes 1179656 | tf_op jit(solution)/shard_map/ppermute | solution.py:44
  374.2 27.2 %collective-permute-start.28 = (bf16[128,1536]{1,0:T(8,128)(2,1)S(1)}, bf16[128,1536]{1,0:T(8,128)(2,1)S(1)}, u32[]{:S(2)}, u32[]{:S(2)}) collective-permute-start(bf16[128,1536]{1,0:T(8,128)(2,1)S(1)} %fusion.1), channel_id=1, source_target_pairs={{0,8},{4,12},{8,16},{12,20},{16,24},{20,28},{24,0},{28,4},{1,9},{5... | collective-permute-start | bytes 1179656 | tf_op jit(solution)/shard_map/ppermute | solution.py:44
  385.0 24.9 %collective-permute-start.118 = (bf16[128,1536]{1,0:T(8,128)(2,1)S(1)}, bf16[128,1536]{1,0:T(8,128)(2,1)S(1)}, u32[]{:S(2)}, u32[]{:S(2)}) collective-permute-start(bf16[128,1536]{1,0:T(8,128)(2,1)S(1)} %add_convert_fusion.1), channel_id=1, source_target_pairs={{0,8},{4,12},{8,16},{12,20},{16,24},{20,28},{24,0},{28,4},{1,9},{5... | collective-permute-start | bytes 1179656 | tf_op jit(solution)/shard_map/ppermute | solution.py:44
  393.4 24.9 %collective-permute-start.75 = (bf16[128,1536]{1,0:T(8,128)(2,1)S(1)}, bf16[128,1536]{1,0:T(8,128)(2,1)S(1)}, u32[]{:S(2)}, u32[]{:S(2)}) collective-permute-start(bf16[128,1536]{1,0:T(8,128)(2,1)S(1)} %add_convert_fusion.5), channel_id=1, source_target_pairs={{0,8},{4,12},{8,16},{12,20},{16,24},{20,28},{24,0},{28,4},{1,9},{5... | collective-permute-start | bytes 1179656 | tf_op jit(solution)/shard_map/ppermute | solution.py:44
  401.8 24.9 %collective-permute-start.29 = (bf16[128,1536]{1,0:T(8,128)(2,1)S(1)}, bf16[128,1536]{1,0:T(8,128)(2,1)S(1)}, u32[]{:S(2)}, u32[]{:S(2)}) collective-permute-start(bf16[128,1536]{1,0:T(8,128)(2,1)S(1)} %add_convert_fusion.9), channel_id=1, source_target_pairs={{0,8},{4,12},{8,16},{12,20},{16,24},{20,28},{24,0},{28,4},{1,9},{5... | collective-permute-start | bytes 1179656 | tf_op jit(solution)/shard_map/ppermute | solution.py:44
  410.2 24.9 %collective-permute-start.119 = (bf16[128,1536]{1,0:T(8,128)(2,1)S(1)}, bf16[128,1536]{1,0:T(8,128)(2,1)S(1)}, u32[]{:S(2)}, u32[]{:S(2)}) collective-permute-start(bf16[128,1536]{1,0:T(8,128)(2,1)S(1)} %add_convert_fusion), channel_id=1, source_target_pairs={{0,8},{4,12},{8,16},{12,20},{16,24},{20,28},{24,0},{28,4},{1,9},{5... | collective-permute-start | bytes 1179656 | tf_op jit(solution)/shard_map/ppermute | solution.py:44
  418.7 24.9 %collective-permute-start.76 = (bf16[128,1536]{1,0:T(8,128)(2,1)S(1)}, bf16[128,1536]{1,0:T(8,128)(2,1)S(1)}, u32[]{:S(2)}, u32[]{:S(2)}) collective-permute-start(bf16[128,1536]{1,0:T(8,128)(2,1)S(1)} %add_convert_fusion.4), channel_id=1, source_target_pairs={{0,8},{4,12},{8,16},{12,20},{16,24},{20,28},{24,0},{28,4},{1,9},{5... | collective-permute-start | bytes 1179656 | tf_op jit(solution)/shard_map/ppermute | solution.py:44
  427.1 24.9 %collective-permute-start.30 = (bf16[128,1536]{1,0:T(8,128)(2,1)S(1)}, bf16[128,1536]{1,0:T(8,128)(2,1)S(1)}, u32[]{:S(2)}, u32[]{:S(2)}) collective-permute-start(bf16[128,1536]{1,0:T(8,128)(2,1)S(1)} %add_convert_fusion.8), channel_id=1, source_target_pairs={{0,8},{4,12},{8,16},{12,20},{16,24},{20,28},{24,0},{28,4},{1,9},{5... | collective-permute-start | bytes 1179656 | tf_op jit(solution)/shard_map/ppermute | solution.py:44
  427.6 31.4 %collective-permute-start.123 = (bf16[128,1280]{1,0:T(8,128)(2,1)S(1)}, bf16[128,1280]{1,0:T(8,128)(2,1)S(1)}, u32[]{:S(2)}, u32[]{:S(2)}) collective-permute-start(bf16[128,1280]{1,0:T(8,128)(2,1)S(1)} %fusion.11), channel_id=1, source_target_pairs={{0,8},{4,12},{8,16},{12,20},{16,24},{20,28},{24,0},{28,4},{1,9},{5... | collective-permute-start | bytes 983048 | tf_op jit(solution)/shard_map/ppermute | solution.py:44
  428.4 104.5 %collective-permute-start.41 = (bf16[768,512]{1,0:T(8,128)(2,1)S(1)}, bf16[768,512]{1,0:T(8,128)(2,1)S(1)}, u32[]{:S(2)}, u32[]{:S(2)}) collective-permute-start(bf16[768,512]{1,0:T(8,128)(2,1)S(1)} %copy-done.17), channel_id=1, source_target_pairs={{0,4},{4,0},{8,12},{12,8},{16,20},{20,16},{24,28},{28,24},{1,5},{5... | collective-permute-start | bytes 2359304 | tf_op jit(solution)/shard_map/ppermute | solution.py:33
  435.1 30.9 %collective-permute-start.80 = (bf16[128,1280]{1,0:T(8,128)(2,1)S(1)}, bf16[128,1280]{1,0:T(8,128)(2,1)S(1)}, u32[]{:S(2)}, u32[]{:S(2)}) collective-permute-start(bf16[128,1280]{1,0:T(8,128)(2,1)S(1)} %fusion.9), channel_id=1, source_target_pairs={{0,8},{4,12},{8,16},{12,20},{16,24},{20,28},{24,0},{28,4},{1,9},{5... | collective-permute-start | bytes 983048 | tf_op jit(solution)/shard_map/ppermute | solution.py:44
  443.5 29.5 %collective-permute-start.35 = (bf16[128,1280]{1,0:T(8,128)(2,1)S(1)}, bf16[128,1280]{1,0:T(8,128)(2,1)S(1)}, u32[]{:S(2)}, u32[]{:S(2)}) collective-permute-start(bf16[128,1280]{1,0:T(8,128)(2,1)S(1)} %fusion.7), channel_id=1, source_target_pairs={{0,8},{4,12},{8,16},{12,20},{16,24},{20,28},{24,0},{28,4},{1,9},{5... | collective-permute-start | bytes 983048 | tf_op jit(solution)/shard_map/ppermute | solution.py:44
  451.9 25.3 %collective-permute-start.120 = (bf16[128,768]{1,0:T(8,128)(2,1)S(1)}, bf16[128,768]{1,0:T(8,128)(2,1)S(1)}, u32[]{:S(2)}, u32[]{:S(2)}) collective-permute-start(bf16[128,768]{1,0:T(8,128)(2,1)S(1)} %get-tuple-element.55), channel_id=1, source_target_pairs={{0,8},{4,12},{8,16},{12,20},{16,24},{20,28},{24,0},{28,4},{1,9},{5... | collective-permute-start | bytes 589832 | tf_op jit(solution)/shard_map/ppermute | solution.py:55
  459.0 22.5 %collective-permute-start.77 = (bf16[128,768]{1,0:T(8,128)(2,1)S(1)}, bf16[128,768]{1,0:T(8,128)(2,1)S(1)}, u32[]{:S(2)}, u32[]{:S(2)}) collective-permute-start(bf16[128,768]{1,0:T(8,128)(2,1)S(1)} %get-tuple-element.67), channel_id=1, source_target_pairs={{0,8},{4,12},{8,16},{12,20},{16,24},{20,28},{24,0},{28,4},{1,9},{5... | collective-permute-start | bytes 589832 | tf_op jit(solution)/shard_map/ppermute | solution.py:55
  466.0 19.7 %collective-permute-start.31 = (bf16[128,768]{1,0:T(8,128)(2,1)S(1)}, bf16[128,768]{1,0:T(8,128)(2,1)S(1)}, u32[]{:S(2)}, u32[]{:S(2)}) collective-permute-start(bf16[128,768]{1,0:T(8,128)(2,1)S(1)} %get-tuple-element.79), channel_id=1, source_target_pairs={{0,8},{4,12},{8,16},{12,20},{16,24},{20,28},{24,0},{28,4},{1,9},{5... | collective-permute-start | bytes 589832 | tf_op jit(solution)/shard_map/ppermute | solution.py:55
  473.0 39.1 %collective-permute-start.124 = (bf16[128,1280]{1,0:T(8,128)(2,1)S(1)}, bf16[128,1280]{1,0:T(8,128)(2,1)S(1)}, u32[]{:S(2)}, u32[]{:S(2)}) collective-permute-start(bf16[128,1280]{1,0:T(8,128)(2,1)S(1)} %add_convert_fusion.13), channel_id=1, source_target_pairs={{0,8},{4,12},{8,16},{12,20},{16,24},{20,28},{24,0},{28,4},{1,9},{5... | collective-permute-start | bytes 983048 | tf_op jit(solution)/shard_map/ppermute | solution.py:44
  477.2 36.4 %collective-permute-start.81 = (bf16[128,1280]{1,0:T(8,128)(2,1)S(1)}, bf16[128,1280]{1,0:T(8,128)(2,1)S(1)}, u32[]{:S(2)}, u32[]{:S(2)}) collective-permute-start(bf16[128,1280]{1,0:T(8,128)(2,1)S(1)} %add_convert_fusion.17), channel_id=1, source_target_pairs={{0,8},{4,12},{8,16},{12,20},{16,24},{20,28},{24,0},{28,4},{1,9},{5... | collective-permute-start | bytes 983048 | tf_op jit(solution)/shard_map/ppermute | solution.py:44
  481.4 22.5 %collective-permute-start.121 = (bf16[128,768]{1,0:T(8,128)(2,1)S(1)}, bf16[128,768]{1,0:T(8,128)(2,1)S(1)}, u32[]{:S(2)}, u32[]{:S(2)}) collective-permute-start(bf16[128,768]{1,0:T(8,128)(2,1)S(1)} %collective-permute-done.120), channel_id=1, source_target_pairs={{0,8},{4,12},{8,16},{12,20},{16,24},{20,28},{24,0},{28,4},{1,9},{5... | collective-permute-start | bytes 589832 | tf_op jit(solution)/shard_map/ppermute | solution.py:55
  485.7 22.2 %collective-permute-start.78 = (bf16[128,768]{1,0:T(8,128)(2,1)S(1)}, bf16[128,768]{1,0:T(8,128)(2,1)S(1)}, u32[]{:S(2)}, u32[]{:S(2)}) collective-permute-start(bf16[128,768]{1,0:T(8,128)(2,1)S(1)} %collective-permute-done.77), channel_id=1, source_target_pairs={{0,8},{4,12},{8,16},{12,20},{16,24},{20,28},{24,0},{28,4},{1,9},{5... | collective-permute-start | bytes 589832 | tf_op jit(solution)/shard_map/ppermute | solution.py:55
  512.1 16.6 %collective-permute-start.79 = (bf16[128,768]{1,0:T(8,128)(2,1)S(1)}, bf16[128,768]{1,0:T(8,128)(2,1)S(1)}, u32[]{:S(2)}, u32[]{:S(2)}) collective-permute-start(bf16[128,768]{1,0:T(8,128)(2,1)S(1)} %collective-permute-done.78), channel_id=1, source_target_pairs={{0,8},{4,12},{8,16},{12,20},{16,24},{20,28},{24,0},{28,4},{1,9},{5... | collective-permute-start | bytes 589832 | tf_op jit(solution)/shard_map/ppermute | solution.py:55
  513.6 19.2 %collective-permute-start.33 = (bf16[128,768]{1,0:T(8,128)(2,1)S(1)}, bf16[128,768]{1,0:T(8,128)(2,1)S(1)}, u32[]{:S(2)}, u32[]{:S(2)}) collective-permute-start(bf16[128,768]{1,0:T(8,128)(2,1)S(1)} %collective-permute-done.32), channel_id=1, source_target_pairs={{0,8},{4,12},{8,16},{12,20},{16,24},{20,28},{24,0},{28,4},{1,9},{5... | collective-permute-start | bytes 589832 | tf_op jit(solution)/shard_map/ppermute | solution.py:55
  520.2 19.7 %collective-permute-start.125 = (bf16[128,1280]{1,0:T(8,128)(2,1)S(1)}, bf16[128,1280]{1,0:T(8,128)(2,1)S(1)}, u32[]{:S(2)}, u32[]{:S(2)}) collective-permute-start(bf16[128,1280]{1,0:T(8,128)(2,1)S(1)} %add_convert_fusion.12), channel_id=1, source_target_pairs={{0,8},{4,12},{8,16},{12,20},{16,24},{20,28},{24,0},{28,4},{1,9},{5... | collective-permute-start | bytes 983048 | tf_op jit(solution)/shard_map/ppermute | solution.py:44
  524.4 22.5 %collective-permute-start.82 = (bf16[128,1280]{1,0:T(8,128)(2,1)S(1)}, bf16[128,1280]{1,0:T(8,128)(2,1)S(1)}, u32[]{:S(2)}, u32[]{:S(2)}) collective-permute-start(bf16[128,1280]{1,0:T(8,128)(2,1)S(1)} %add_convert_fusion.16), channel_id=1, source_target_pairs={{0,8},{4,12},{8,16},{12,20},{16,24},{20,28},{24,0},{28,4},{1,9},{5... | collective-permute-start | bytes 983048 | tf_op jit(solution)/shard_map/ppermute | solution.py:44
  528.6 25.3 %collective-permute-start.37 = (bf16[128,1280]{1,0:T(8,128)(2,1)S(1)}, bf16[128,1280]{1,0:T(8,128)(2,1)S(1)}, u32[]{:S(2)}, u32[]{:S(2)}) collective-permute-start(bf16[128,1280]{1,0:T(8,128)(2,1)S(1)} %add_convert_fusion.20), channel_id=1, source_target_pairs={{0,8},{4,12},{8,16},{12,20},{16,24},{20,28},{24,0},{28,4},{1,9},{5... | collective-permute-start | bytes 983048 | tf_op jit(solution)/shard_map/ppermute | solution.py:44
  532.9 46.3 %collective-permute-start.42 = (bf16[640,512]{1,0:T(8,128)(2,1)S(1)}, bf16[640,512]{1,0:T(8,128)(2,1)S(1)}, u32[]{:S(2)}, u32[]{:S(2)}) collective-permute-start(bf16[640,512]{1,0:T(8,128)(2,1)S(1)} %copy-done.21), channel_id=1, source_target_pairs={{0,4},{4,0},{8,12},{12,8},{16,20},{20,16},{24,28},{28,24},{1,5},{5... | collective-permute-start | bytes 1966088 | tf_op jit(solution)/shard_map/ppermute | solution.py:33
  540.4 17.0 %collective-permute-start.126 = (bf16[128,640]{1,0:T(8,128)(2,1)S(1)}, bf16[128,640]{1,0:T(8,128)(2,1)S(1)}, u32[]{:S(2)}, u32[]{:S(2)}) collective-permute-start(bf16[128,640]{1,0:T(8,128)(2,1)S(1)} %get-tuple-element.57), channel_id=1, source_target_pairs={{0,8},{4,12},{8,16},{12,20},{16,24},{20,28},{24,0},{28,4},{1,9},{5... | collective-permute-start | bytes 491528 | tf_op jit(solution)/shard_map/ppermute | solution.py:55
  547.5 13.5 %collective-permute-start.83 = (bf16[128,640]{1,0:T(8,128)(2,1)S(1)}, bf16[128,640]{1,0:T(8,128)(2,1)S(1)}, u32[]{:S(2)}, u32[]{:S(2)}) collective-permute-start(bf16[128,640]{1,0:T(8,128)(2,1)S(1)} %get-tuple-element.69), channel_id=1, source_target_pairs={{0,8},{4,12},{8,16},{12,20},{16,24},{20,28},{24,0},{28,4},{1,9},{5... | collective-permute-start | bytes 491528 | tf_op jit(solution)/shard_map/ppermute | solution.py:55
  590.7 17.0 %collective-permute-start.44 = (bf16[128,1024]{0,1:T(8,128)(2,1)S(1)}, bf16[128,1024]{0,1:T(8,128)(2,1)S(1)}, u32[]{:S(2)}, u32[]{:S(2)}) collective-permute-start(bf16[128,1024]{0,1:T(8,128)(2,1)S(1)} %dynamic-slice_convert_fusion.4), channel_id=1, source_target_pairs={{0,2},{1,3},{2,0},{3,1},{4,6},{5,7},{6,4},{7,5},{8,10},{9,11},{10,... | collective-permute-start | bytes 786440 | tf_op jit(solution)/shard_map/ppermute | solution.py:44
  (112 other events, 925.5 us)
where the time goes:
time: 652 us; the launch traced here: 643 us
  waiting for transfers between devices  450 us (69%)
  starting transfers between devices  75.3 us (12%)
  matrix products  65.8 us (10%)
  local copies, waits for them, and re-layouts  35.7 us (5%)
  other arithmetic  13.2 us (2%)
    ppermute x42, waiting for transfers between devices, ring_reduce(): arrived = lax.ppermute(total.astype(BF16), axis, perm)  254 us
    ppermute x42, waiting for transfers between devices, ring_gather(): x = lax.ppermute(x, axis, perm)  163 us
    dot_general x120, matrix products, dot(): return jnp.dot(a, b, preferred_element_type=F32)  65.8 us
    ppermute x35, waiting for transfers between devices, swap(): return lax.ppermute(x, axis, xor_perm(lax.axis_size(axis), 1))  25.6 us
    ppermute x35, starting transfers between devices, swap(): return lax.ppermute(x, axis, xor_perm(lax.axis_size(axis), 1))  21.6 us
    ppermute x18, starting transfers between devices, sum_over_ra(): stats = stats + lax.ppermute(stats, 'ra', xor_perm(total, bit))  20.8 us
    ppermute x42, starting transfers between devices, ring_reduce(): arrived = lax.ppermute(total.astype(BF16), axis, perm)  19.8 us
    ppermute x42, starting transfers between devices, ring_gather(): x = lax.ppermute(x, axis, perm)  13.2 us
  transfers between devices with their start and end apart: 137, of which 91 were waited for; matrix products, arithmetic and copies ran while one was open for 16% of the time, Pallas kernels for 0%

commit v1 on v0

--- a/solution.py
+++ b/solution.py
@@ -1,6 +1,10 @@
+import functools
+
 import jax
 import jax.numpy as jnp
 from jax import lax
+from jax.experimental import pallas as pl
+from jax.experimental.pallas import tpu as pltpu
 from jax.sharding import PartitionSpec as P
 
 LAYERS = 2
@@ -170,9 +174,566 @@
     return jnp.concatenate(streams, axis=0)
 
 
+UNIT = 128
+TOKEN_PARTS = 3
+HOP = 2
+IN_FLIGHT = 4
+MESH_ID = pl.DeviceIdType.MESH
+
+
+def layer_kernel(
+    groups, x_hbm, gate_hbm, up_hbm, down_hbm, gain, shift, out_hbm,
+    wgu, wd, stream, sums, hid, acc, core_out, core_in, y_out, y_in, x_out, x_in, stat_out, stat_in,
+    own_sem, wgu_send, wgu_recv, wd_send, wd_recv, sum_send, sum_recv, hid_send, hid_recv,
+    core_send, core_recv, y_send, y_recv, x_send, x_recv, stat_send, stat_recv,
+    xg_send, xg_recv, yg_send, yg_recv, cg_send, cg_recv, out_sem,
+):
+    n_ra = 2 * groups
+    tokens, width = x_hbm.shape
+    full_width = width * n_ra
+    layers, nc = wgu.shape[0], wgu.shape[1]
+    nt = acc.shape[0] // 2
+    rows = acc.shape[1]
+    half_rows, quarter = rows // 2, rows // 4
+    used = nc * nt
+    steps = used + layer_gap(groups, nc, nt)
+    total = layers * steps
+    units = nc * UNIT
+
+    r, c = lax.axis_index("ra"), lax.axis_index("cb")
+    q, g = lax.rem(r, 2), r // 2
+    core, y = lax.rem(c, 2), c // 2
+    x_peer = (r + 1 - 2 * q, c)
+    y_peer = (r, (1 - y) * 2 + core)
+    core_peer = (r, y * 2 + 1 - core)
+
+    def place(h):
+        p = (groups - 1 - g) if h == 0 else g
+        ahead = (r - 2, c) if h == 0 else (r + 2, c)
+        back = (r + 2, c) if h == 0 else (r - 2, c)
+        return p, ahead, back
+
+    def remote(src, dst, send, recv, to):
+        return pltpu.make_async_remote_copy(src_ref=src, dst_ref=dst, send_sem=send, recv_sem=recv, device_id=to, device_id_type=MESH_ID)
+
+    pairs = nc // 2
+    odd = nc - 2 * pairs
+
+    def order(n):
+        layer = n // steps
+        j = n - layer * steps
+        first = layer == 0
+        b, k = j // 3, lax.rem(j, 3)
+        j3 = j - 3 * pairs - odd
+        j4 = j3 - (nc - pairs)
+        t_a = jnp.where(k == 2, 1, 0)
+        c_a = jnp.where(k == 2, b, 2 * b + k)
+        t_c = jnp.where(j4 < 0, 1, 2 + j4 // nc)
+        c_c = jnp.where(j4 < 0, pairs + j3, lax.rem(jnp.maximum(j4, 0), nc))
+        t_b = jnp.where(j3 < 0, 0, t_c)
+        c_b = jnp.where(j3 < 0, nc - 1, c_c)
+        t0 = jnp.where(j < 3 * pairs, t_a, t_b)
+        c0 = jnp.where(j < 3 * pairs, c_a, c_b)
+        t = jnp.where(first, t0, j // nc)
+        cc = jnp.where(first, c0, lax.rem(j, nc))
+        return layer, t, cc
+
+    def valid(n):
+        return (n >= 0) & (n < total) & (lax.rem(jnp.maximum(n, 0), steps) < used)
+
+    def row_of(h, t):
+        return pl.multiple_of(h * (nt * rows) + t * rows, rows)
+
+    def rows_at(start, size):
+        return pl.ds(pl.multiple_of(start, quarter), size)
+
+    def gu_copy(layer, cc, which):
+        src = gate_hbm if which == 0 else up_hbm
+        cols = pl.ds(pl.multiple_of((1 - q) * units + cc * UNIT, UNIT), UNIT)
+        return remote(
+            src.at[layer, :, cols],
+            wgu.at[layer, cc, pl.ds(width, width), pl.ds(which * UNIT, UNIT)],
+            wgu_send.at[layer, cc, which], wgu_recv.at[layer, cc, which], x_peer,
+        )
+
+    def d_copy(layer, cc):
+        src_rows = pl.ds(pl.multiple_of((1 - q) * units + cc * UNIT, UNIT), UNIT)
+        return remote(
+            down_hbm.at[layer, src_rows, :],
+            wd.at[layer, cc, :, pl.ds(width, width)],
+            wd_send.at[layer, cc], wd_recv.at[layer, cc], x_peer,
+        )
+
+    def send_gu(layer, cc):
+        gu_copy(layer, cc, 0).start()
+        gu_copy(layer, cc, 1).start()
+
+    def own_gu(layer, cc, which):
+        src = gate_hbm if which == 0 else up_hbm
+        cols = pl.ds(pl.multiple_of(q * units + cc * UNIT, UNIT), UNIT)
+        return pltpu.make_async_copy(
+            src.at[layer, :, cols], wgu.at[layer, cc, pl.ds(0, width), pl.ds(which * UNIT, UNIT)], own_sem.at[0, layer, cc, which]
+        )
+
+    def own_d(layer, cc):
+        src_rows = pl.ds(pl.multiple_of(q * units + cc * UNIT, UNIT), UNIT)
+        return pltpu.make_async_copy(down_hbm.at[layer, src_rows, :], wd.at[layer, cc, :, pl.ds(0, width)], own_sem.at[1, layer, cc, 0])
+
+    own_x = pltpu.make_async_copy(x_hbm, stream.at[:, pl.ds(0, width)], out_sem.at[0])
+
+    other_cols = pl.ds(width, width)
+
+    def first_x(h, t):
+        mine = rows_at(row_of(h, t) + core * half_rows + y * quarter, quarter)
+        return remote(x_hbm.at[mine, :], stream.at[mine, other_cols], xg_send.at[h, t], xg_recv.at[h, t], x_peer)
+
+    def first_y(h, t):
+        mine = rows_at(row_of(h, t) + core * half_rows + y * quarter, quarter)
+        view = stream.at[mine, other_cols]
+        return remote(view, view, yg_send.at[h, t], yg_recv.at[h, t], y_peer)
+
+    def first_core(h, t):
+        mine = rows_at(row_of(h, t) + core * half_rows, half_rows)
+        view = stream.at[mine, other_cols]
+        return remote(view, view, cg_send.at[h, t], cg_recv.at[h, t], core_peer)
+
+    for t in range(nt):
+        for h in range(2):
+            first_x(h, t).start()
+        if t == 0:
+            own_x.start()
+            send_gu(0, 0)
+    for cc in range(1, min(IN_FLIGHT, nc)):
+        send_gu(0, cc)
+
+    def own_start(j, _):
+        layer, cc = j // nc, lax.rem(j, nc)
+        own_gu(layer, cc, 0).start()
+        own_gu(layer, cc, 1).start()
+        own_d(layer, cc).start()
+        return 0
+
+    def own_wait(j, _):
+        layer, cc = j // nc, lax.rem(j, nc)
+        own_gu(layer, cc, 0).wait()
+        own_gu(layer, cc, 1).wait()
+        own_d(layer, cc).wait()
+        return 0
+
+    lax.fori_loop(0, layers * nc, own_start, 0)
+    for t in range(nt):
+        for h in range(2):
+            first_x(h, t).wait_recv()
+            first_y(h, t).start()
+    own_x.wait()
+    for t in range(nt):
+        for h in range(2):
+            first_y(h, t).wait_recv()
+            first_core(h, t).start()
+    lax.fori_loop(0, layers * nc, own_wait, 0)
+    for t in range(nt):
+        for h in range(2):
+            first_x(h, t).wait_send()
+            first_y(h, t).wait_send()
+            first_core(h, t).wait_send()
+
+    def sum_copy(h, n):
+        _, t, cc = order(n)
+        _, ahead, _ = place(h)
+        view = sums.at[h, t * nc + cc]
+        return remote(view, view, sum_send.at[h, lax.rem(n, 4)], sum_recv.at[h, t * nc + cc], ahead)
+
+    def hid_copy(h, n):
+        _, t, cc = order(n)
+        _, _, back = place(h)
+        view = hid.at[h, t * nc + cc]
+        return remote(view, view, hid_send.at[h, lax.rem(n, 4)], hid_recv.at[h, t * nc + cc], back)
+
+    def stage_sum(h, n):
+        p, _, _ = place(h)
+        layer, t, cc = order(n)
+
+        @pl.when((cc == 0) & (layer == 0))
+        def _():
+            first_core(h, t).wait_recv()
+
+        @pl.when((cc == 0) & (layer > 0))
+        def _():
+            gather_core(h, t).wait_recv()
+
+        slot = t * nc + cc
+        own = jnp.dot(stream[pl.ds(row_of(h, t), rows), :], wgu[layer, cc], preferred_element_type=F32)
+
+        @pl.when(p == 0)
+        def _():
+            sums[h, slot] = own.astype(BF16)
+
+        @pl.when((p > 0) & (p < groups - 1))
+        def _():
+            sum_copy(h, n).wait_recv()
+            sums[h, slot] = (sums[h, slot].astype(F32) + own).astype(BF16)
+
+        @pl.when(p < groups - 1)
+        def _():
+            sum_copy(h, n).start()
+
+        @pl.when(p == groups - 1)
+        def _():
+            sum_copy(h, n).wait_recv()
+            whole = sums[h, slot].astype(F32) + own
+            hid[h, slot] = (jax.nn.silu(whole[:, :UNIT]) * whole[:, UNIT:]).astype(BF16)
+
+    def stage_hid(h, n):
+        p, _, _ = place(h)
+
+        @pl.when(p < groups - 1)
+        def _():
+            hid_copy(h, n).wait_recv()
+
+        @pl.when(p > 0)
+        def _():
+            hid_copy(h, n).start()
+
+    def stage_down(h, n):
+        layer, t, cc = order(n)
+        part_sum = jnp.dot(hid[h, t * nc + cc], wd[layer, cc], preferred_element_type=F32)
+        m = h * nt + t
+
+        @pl.when(cc == 0)
+        def _():
+            acc[m] = part_sum
+
+        @pl.when(cc > 0)
+        def _():
+            acc[m] += part_sum
+
+    def core_copy(h, t):
+        m = h * nt + t
+        return remote(core_out.at[m], core_in.at[m], core_send.at[h, t], core_recv.at[h, t], core_peer)
+
+    def y_copy(h, t):
+        m = h * nt + t
+        return remote(y_out.at[m], y_in.at[m], y_send.at[h, t], y_recv.at[h, t], y_peer)
+
+    def x_copy(h, t):
+        m = h * nt + t
+        return remote(x_out.at[m], x_in.at[m], x_send.at[h, t], x_recv.at[h, t], x_peer)
+
+    def stat_copy(h, t, k):
+        m = h * nt + t
+        return remote(stat_out.at[m], stat_in.at[m, k], stat_send.at[h, t, k], stat_recv.at[h, t, k], (lax.rem(r + k, n_ra), c))
+
+    def gather_x(h, t):
+        mine = rows_at(row_of(h, t) + core * half_rows + y * quarter, quarter)
+        return remote(stream.at[mine, pl.ds(0, width)], stream.at[mine, other_cols], xg_send.at[h, t], xg_recv.at[h, t], x_peer)
+
+    def gather_y(h, t):
+        mine = rows_at(row_of(h, t) + core * half_rows + y * quarter, quarter)
+        return remote(stream.at[mine, :], stream.at[mine, :], yg_send.at[h, t], yg_recv.at[h, t], y_peer)
+
+    def gather_core(h, t):
+        mine = rows_at(row_of(h, t) + core * half_rows, half_rows)
+        return remote(stream.at[mine, :], stream.at[mine, :], cg_send.at[h, t], cg_recv.at[h, t], core_peer)
+
+    def out_copy(h, t):
+        at = pl.ds(row_of(h, t), rows)
+        return pltpu.make_async_copy(stream.at[at, pl.ds(0, width)], out_hbm.at[at, :], out_sem.at[1 + h * nt + t])
+
+    kept_half = pl.multiple_of(core * half_rows, half_rows)
+    sent_half = pl.multiple_of((1 - core) * half_rows, half_rows)
+    kept = pl.multiple_of(core * half_rows + y * quarter, quarter)
+    sent = pl.multiple_of(core * half_rows + (1 - y) * quarter, quarter)
+
+    def end_core(h, layer, t):
+        m = h * nt + t
+        core_out[m] = acc[m, pl.ds(sent_half, half_rows), :].astype(BF16)
+        core_copy(h, t).start()
+
+    def end_y(h, layer, t):
+        m = h * nt + t
+        core_copy(h, t).wait()
+        acc[m, pl.ds(kept_half, half_rows), :] += core_in[m].astype(F32)
+        y_out[m] = acc[m, pl.ds(sent, quarter), :].astype(BF16)
+        y_copy(h, t).start()
+
+    def end_x(h, layer, t):
+        m = h * nt + t
+        y_copy(h, t).wait()
+        acc[m, pl.ds(kept, quarter), :] += y_in[m].astype(F32)
+        x_out[m] = acc[m, pl.ds(kept, quarter), pl.ds(width, width)].astype(BF16)
+        x_copy(h, t).start()
+
+    def lane_fold(v):
+        total_v = v[:, :UNIT]
+        for at in range(UNIT, width, UNIT):
+            total_v = total_v + v[:, at:at + UNIT]
+        return total_v
+
+    def across(a, b):
+        return lax.dot_general(a, b, (((1,), (1,)), ((), ())), preferred_element_type=F32, precision=lax.Precision.HIGHEST)
+
+    def end_stats(h, layer, t):
+        m = h * nt + t
+        x_copy(h, t).wait()
+        branch = acc[m, pl.ds(kept, quarter), pl.ds(0, width)] + x_in[m].astype(F32)
+        mine = stream[rows_at(row_of(h, t) + kept, quarter), pl.ds(0, width)]
+        mixed = RESIDUAL * mine.astype(F32) + branch
+        acc[m, pl.ds(kept, quarter), pl.ds(0, width)] = mixed
+        ones = jnp.ones((8, UNIT), F32)
+        plain = across(ones, lane_fold(mixed))
+        squared = across(ones, lane_fold(mixed * mixed))
+        at = lax.broadcasted_iota(jnp.int32, plain.shape, 0)
+        stat_out[m] = jnp.where(at < 4, plain, squared)
+        for k in range(1, n_ra):
+            stat_copy(h, t, k).start()
+
+    def end_norm(h, layer, t):
+        m = h * nt + t
+        whole = stat_out[m]
+        for k in range(1, n_ra):
+            stat_copy(h, t, k).wait()
+            whole = whole + stat_in[m, k]
+        eye = (lax.broadcasted_iota(jnp.int32, (quarter, quarter), 0) == lax.broadcasted_iota(jnp.int32, (quarter, quarter), 1)).astype(F32)
+        turned = across(eye, whole)
+        mean = turned[:, 0:1] / full_width
+        var = turned[:, 4:5] / full_width - mean * mean
+        mixed = acc[m, pl.ds(kept, quarter), pl.ds(0, width)]
+        normed = (mixed - mean) * lax.rsqrt(var + EPSILON)
+        normed = normed * gain[pl.ds(layer, 1), :] + shift[pl.ds(layer, 1), :]
+        stream[rows_at(row_of(h, t) + kept, quarter), pl.ds(0, width)] = normed.astype(BF16)
+
+        @pl.when(layer < layers - 1)
+        def _():
+            gather_x(h, t).start()
+
+    def end_gather_y(h, layer, t):
+        @pl.when(layer < layers - 1)
+        def _():
+            gather_x(h, t).wait()
+
+        gather_y(h, t).start()
+
+    def end_gather_core(h, layer, t):
+        gather_y(h, t).wait()
+        gather_core(h, t).start()
+
+    def end_sent(h, layer, t):
+        gather_core(h, t).wait_send()
+
+        @pl.when(layer == layers - 1)
+        def _():
+            gather_core(h, t).wait_recv()
+            out_copy(h, t).start()
+
+    longest = HOP * 2 * (groups - 1)
+
+    def lag_hid(h):
+        return longest - HOP * place(h)[0]
+
+    stages = (
+        (lambda h: lag_hid(h), end_core),
+        (lambda h: lag_hid(h) + ENDS[0], end_y),
+        (lambda h: lag_hid(h) + ENDS[1], end_x),
+        (lambda h: lag_hid(h) + ENDS[2], end_stats),
+        (lambda h: longest + ENDS[3], end_norm),
+        (lambda h: longest + ENDS[4], end_gather_y),
+        (lambda h: longest + ENDS[5], end_gather_core),
+        (lambda h: longest + ENDS[6], end_sent),
+    )
+
+    p0, p1 = place(0)[0], place(1)[0]
+    p_low, p_high = jnp.minimum(p0, p1), jnp.maximum(p0, p1)
+
+    def weight_message(w):
+        layer = w // (2 * nc)
+        k = w - layer * 2 * nc
+        lead = jnp.where(layer == 0, IN_FLIGHT, 1)
+        mid = k - lead
+        in_mid = (mid >= 0) & (mid < 2 * (nc - lead))
+        is_gu = (k < lead) | (in_mid & (lax.rem(jnp.maximum(mid, 0), 2) == 1))
+        gu_at = jnp.where(k < lead, k, lead + mid // 2)
+        d_at = jnp.where(in_mid, mid // 2, k - nc)
+        return layer, is_gu, gu_at, d_at
+
+    n_messages = 2 * nc * layers
+
+    def issue_weights(w):
+        layer, is_gu, gu_at, d_at = weight_message(w)
+
+        @pl.when(is_gu)
+        def _():
+            send_gu(layer, gu_at)
+
+        @pl.when(jnp.logical_not(is_gu))
+        def _():
+            d_copy(layer, d_at).start()
+
+    def sent_weights(w):
+        layer, is_gu, gu_at, d_at = weight_message(w)
+
+        @pl.when(is_gu)
+        def _():
+            gu_copy(layer, gu_at, 0).wait_send()
+            gu_copy(layer, gu_at, 1).wait_send()
+
+        @pl.when(jnp.logical_not(is_gu))
+        def _():
+            d_copy(layer, d_at).wait_send()
+
+    fast = 2 * nc - IN_FLIGHT
+
+    def body(i, _):
+        j = i - fast
+        slow = (j >= 0) & (lax.rem(jnp.maximum(j, 0), 5) < 4)
+        w = jnp.where(j < 0, IN_FLIGHT + i, 2 * nc + (j // 5) * 4 + lax.rem(jnp.maximum(j, 0), 5))
+
+        @pl.when(((j < 0) | slow) & (w < n_messages))
+        def _():
+            sent_weights(w - IN_FLIGHT)
+            issue_weights(w)
+
+        n_w = i - HOP * p_low
+        layer_w, t_w, c_w = order(n_w)
+
+        @pl.when(valid(n_w) & (t_w == 0))
+        def _():
+            gu_copy(layer_w, c_w, 0).wait_recv()
+            gu_copy(layer_w, c_w, 1).wait_recv()
+
+        n_d = i - longest + HOP * p_high
+        layer_d, t_d, c_d = order(n_d)
+
+        @pl.when(valid(n_d) & (t_d == 0))
+        def _():
+            d_copy(layer_d, c_d).wait_recv()
+
+        for h in range(2):
+            p, _, _ = place(h)
+            n_s = i - HOP * p
+            n_h = i - lag_hid(h)
+
+            @pl.when(valid(n_s - 2) & (p < groups - 1))
+            def _(h=h, n=n_s - 2):
+                sum_copy(h, n).wait_send()
+
+            @pl.when(valid(n_h - 2) & (p > 0))
+            def _(h=h, n=n_h - 2):
+                hid_copy(h, n).wait_send()
+
+            @pl.when(valid(n_h) & (p < groups - 1))
+            def _(h=h, n=n_h):
+                stage_hid(h, n)
+
+        for h in range(2):
+            p, _, _ = place(h)
+            n_s = i - HOP * p
+
+            @pl.when(valid(n_s))
+            def _(h=h, n=n_s):
+                stage_sum(h, n)
+
+            @pl.when(valid(n_s) & (p == groups - 1))
+            def _(h=h, n=n_s):
+                stage_hid(h, n)
+
+        for h in range(2):
+            n_h = i - lag_hid(h)
+
+            @pl.when(valid(n_h))
+            def _(h=h, n=n_h):
+                stage_down(h, n)
+
+        for lag, stage in stages:
+            for h in range(2):
+                n_e = i - lag(h)
+                layer_e, t_e, c_e = order(n_e)
+
+                @pl.when(valid(n_e) & (c_e == nc - 1))
+                def _(h=h, stage=stage, layer_e=layer_e, t_e=t_e):
+                    stage(h, layer_e, t_e)
+
+        return 0
+
+    lax.fori_loop(0, total + longest + ENDS[6], body, 0)
+    for w in range(n_messages - IN_FLIGHT, n_messages):
+        sent_weights(jnp.int32(w))
+    for t in range(nt):
+        for h in range(2):
+            out_copy(h, t).wait()
+
+
+ENDS = (1, 3, 5, 7, 9, 11, 12)
+
+
+def layer_gap(groups, nc, nt):
+    after = HOP * 2 * (groups - 1) + ENDS[5] + 1
+    pairs = nc // 2
+    ends = [2 * pairs + pairs - 2 if nc == 2 * pairs else 3 * pairs]
+    ends += [3 * pairs + (nc - 2 * pairs) + (nc - pairs) - 1]
+    ends += [t * nc + nc - 1 for t in range(2, nt)]
+    return max([0] + [ends[t] + after - (nc * nt + t * nc) for t in range(nt)])
+
+
+def fits(ra, cb, tokens, width, columns):
+    units = columns // PAIR
+    return (
+        ra % PAIR == 0 and ra >= 2 * PAIR and cb == 4 and units % UNIT == 0 and units // UNIT > IN_FLIGHT
+        and width % UNIT == 0 and tokens % (2 * TOKEN_PARTS * 4 * 16) == 0
+    )
+
+
+def per_device_kernel(inputs, gate_weight, up_weight, down_weight, norm_gain, norm_shift):
+    ra = lax.axis_size("ra")
+    tokens, width = inputs.shape
+    layers, _, columns = gate_weight.shape
+    groups, units = ra // PAIR, columns // PAIR
+    nc, nt = units // UNIT, TOKEN_PARTS
+    rows = tokens // (2 * nt)
+    slots, chunks = nc * nt, 2 * nt
+    dma = pltpu.SemaphoreType.DMA
+    scratch = [
+        pltpu.VMEM((layers, nc, 2 * width, 2 * UNIT), BF16),
+        pltpu.VMEM((layers, nc, UNIT, 2 * width), BF16),
+        pltpu.VMEM((tokens, 2 * width), BF16),
+        pltpu.VMEM((2, slots, rows, 2 * UNIT), BF16),
+        pltpu.VMEM((2, slots, rows, UNIT), BF16),
+        pltpu.VMEM((chunks, rows, 2 * width), F32),
+        pltpu.VMEM((chunks, rows // 2, 2 * width), BF16),
+        pltpu.VMEM((chunks, rows // 2, 2 * width), BF16),
+        pltpu.VMEM((chunks, rows // 4, 2 * width), BF16),
+        pltpu.VMEM((chunks, rows // 4, 2 * width), BF16),
+        pltpu.VMEM((chunks, rows // 4, width), BF16),
+        pltpu.VMEM((chunks, rows // 4, width), BF16),
+        pltpu.VMEM((chunks, 8, rows // 4), F32),
+        pltpu.VMEM((chunks, ra, 8, rows // 4), F32),
+        dma((2, layers, nc, 2)),
+        dma((layers, nc, 2)), dma((layers, nc, 2)), dma((layers, nc)), dma((layers, nc)),
+        dma((2, 4)), dma((2, slots)), dma((2, 4)), dma((2, slots)),
+        dma((2, nt)), dma((2, nt)), dma((2, nt)), dma((2, nt)), dma((2, nt)), dma((2, nt)),
+        dma((2, nt, ra)), dma((2, nt, ra)),
+        dma((2, nt)), dma((2, nt)), dma((2, nt)), dma((2, nt)), dma((2, nt)), dma((2, nt)),
+        dma((1 + chunks,)),
+    ]
+    anywhere, near = pl.BlockSpec(memory_space=pl.ANY), pl.BlockSpec(memory_space=pltpu.VMEM)
+    return pl.pallas_call(
+        functools.partial(layer_kernel, groups),
+        out_shape=jax.ShapeDtypeStruct((tokens, width), BF16),
+        in_specs=[anywhere] * 4 + [near] * 2,
+        out_specs=anywhere,
+        scratch_shapes=scratch,
+        compiler_params=pltpu.CompilerParams(has_side_effects=True, vmem_limit_bytes=62 * 2**20),
+    )(inputs, gate_weight, up_weight, down_weight, norm_gain, norm_shift)
+
+
+def per_device_any(inputs, gate_weight, up_weight, down_weight, norm_gain, norm_shift):
+    ra, cb = lax.axis_size("ra"), lax.axis_size("cb")
+    run = per_device_kernel if fits(ra, cb, *inputs.shape, gate_weight.shape[2]) else per_device
+    return run(inputs, gate_weight, up_weight, down_weight, norm_gain, norm_shift)
+
+
 def solution(mesh):
     return jax.shard_map(
-        per_device,
+        per_device_any,
         mesh=mesh,
         in_specs=(
             P(None, "ra"),

time: 652 us -> 399 us (0.61); the launches traced: 643 us -> 399 us
  waiting for transfers between devices: 450 us -> 0 us
  Pallas kernels: 0 us -> 396 us
  starting transfers between devices: 75.3 us -> 0 us
  matrix products: 65.8 us -> 0 us
  local copies, waits for them, and re-layouts: 35.7 us -> 2.65 us
  other arithmetic: 13.2 us -> 0 us
    ppermute x137 -> x0, waiting for transfers between devices: 450 us -> none  [the longest x42 254 us: ring_reduce(): arrived = lax.ppermute(total.astype(BF16), axis, perm)]
    pallas_call x0 -> x1, Pallas kernels: none -> 396 us  [per_device_kernel(): pl.pallas_call(functools.partial(layer_kernel, groups), out_shape=jax.Sha...]
    ppermute x137 -> x0, starting transfers between devices: 75.3 us -> none  [the longest x35 21.6 us: swap(): return lax.ppermute(x, axis, xor_perm(lax.axis_size(axis), 1))]
    dot_general x120 -> x0, matrix products: 65.8 us -> none  [dot(): return jnp.dot(a, b, preferred_element_type=F32)]
    squeeze x4 -> x0, local copies, waits for them, and re-layouts: 14.8 us -> none  [the longest x2 5.17 us: weights_of(): lax.dynamic_slice(down_weight, (layer, sent + start, 0), (1, size, width))]
  transfers between devices with their start and end apart: 137 -> 0, of which waited for: 91 -> 0; matrix products, arithmetic and copies ran while one was open for 16% -> 0% of each run, Pallas kernels for 0% -> 0%
where the time goes in v1:
time: 399 us
  Pallas kernels  396 us (99%)
    pallas_call x1, Pallas kernels, per_device_kernel(): pl.pallas_call(functools.partial(layer_kernel, groups), out_shape=jax.Sha...  396 us

profile of v1, /device:TPU:0, one launch (start us, length us, event | category | flops | bytes accessed | tf_op | source)
XLA Modules:
  0.0 399.1 jit_solution(16506203308304511095)
XLA Ops:
  0.0 396.4 %shard_map.64 = bf16[1536,512]{1,0:T(8,128)(2,1)} custom-call(bf16[1536,512]{1,0:T(8,128)(2,1)} %x_hbm.1, bf16[2,512,2816]{2,1,0:T(8,128)(2,1)} %gate_hbm.1, bf16[2,512,2816]{2,1,0:T(8,128)(2,1)} %up_hbm.1, bf16[2,2816,512]{2,1,0:T(8,128)(2,1)} %down_hbm.1, f32[2,512]{1,0:T(2,128)} %gain.1, f32[2,512]{1,0:T(2,128)} %shift.1), custom_call_target="tpu_custom_call" | custom-call | tf_op jit(solution)/shard_map/pallas_call | solution.py:718
  396.4 2.7 copy.8

commit v2 on v1

--- a/solution.py
+++ b/solution.py
@@ -176,17 +176,24 @@
 
 UNIT = 128
 TOKEN_PARTS = 3
-HOP = 2
+HOP = 3
+BACK = 3
+SENT = 4
+LEAD = 2
+AHEAD = 6
 IN_FLIGHT = 4
+EARLY_OF = 4
+LATE_OF = 7
+LATE = (6, 10, 14)
 MESH_ID = pl.DeviceIdType.MESH
 
 
 def layer_kernel(
     groups, x_hbm, gate_hbm, up_hbm, down_hbm, gain, shift, out_hbm,
-    wgu, wd, stream, sums, hid, acc, core_out, core_in, y_out, y_in, x_out, x_in, stat_out, stat_in,
+    wgu, wd, stream, sums, hid, acc, core_out, core_in, plane_out, plane_in, stat_out, stat_in,
     own_sem, wgu_send, wgu_recv, wd_send, wd_recv, sum_send, sum_recv, hid_send, hid_recv,
-    core_send, core_recv, y_send, y_recv, x_send, x_recv, stat_send, stat_recv,
-    xg_send, xg_recv, yg_send, yg_recv, cg_send, cg_recv, out_sem,
+    core_send, core_recv, plane_send, plane_recv, stat_send, stat_recv,
+    xg_send, xg_recv, yg_send, yg_recv, dg_send, dg_recv, cg_send, cg_recv, out_sem,
 ):
     n_ra = 2 * groups
     tokens, width = x_hbm.shape
@@ -196,8 +203,7 @@
     rows = acc.shape[1]
     half_rows, quarter = rows // 2, rows // 4
     used = nc * nt
-    steps = used + layer_gap(groups, nc, nt)
-    total = layers * steps
+    steps = 2 * used + layer_gap(groups, nc, nt)
     units = nc * UNIT
 
     r, c = lax.axis_index("ra"), lax.axis_index("cb")
@@ -206,6 +212,7 @@
     x_peer = (r + 1 - 2 * q, c)
     y_peer = (r, (1 - y) * 2 + core)
     core_peer = (r, y * 2 + 1 - core)
+    far_peer = (x_peer[0], y_peer[1])
 
     def place(h):
         p = (groups - 1 - g) if h == 0 else g
@@ -216,30 +223,15 @@
     def remote(src, dst, send, recv, to):
         return pltpu.make_async_remote_copy(src_ref=src, dst_ref=dst, send_sem=send, recv_sem=recv, device_id=to, device_id_type=MESH_ID)
 
-    pairs = nc // 2
-    odd = nc - 2 * pairs
-
-    def order(n):
-        layer = n // steps
-        j = n - layer * steps
-        first = layer == 0
-        b, k = j // 3, lax.rem(j, 3)
-        j3 = j - 3 * pairs - odd
-        j4 = j3 - (nc - pairs)
-        t_a = jnp.where(k == 2, 1, 0)
-        c_a = jnp.where(k == 2, b, 2 * b + k)
-        t_c = jnp.where(j4 < 0, 1, 2 + j4 // nc)
-        c_c = jnp.where(j4 < 0, pairs + j3, lax.rem(jnp.maximum(j4, 0), nc))
-        t_b = jnp.where(j3 < 0, 0, t_c)
-        c_b = jnp.where(j3 < 0, nc - 1, c_c)
-        t0 = jnp.where(j < 3 * pairs, t_a, t_b)
-        c0 = jnp.where(j < 3 * pairs, c_a, c_b)
-        t = jnp.where(first, t0, j // nc)
-        cc = jnp.where(first, c0, lax.rem(j, nc))
-        return layer, t, cc
-
-    def valid(n):
-        return (n >= 0) & (n < total) & (lax.rem(jnp.maximum(n, 0), steps) < used)
+    def order(j):
+        both = j < 2 * nc
+        return jnp.where(both, lax.rem(j, 2), j // nc), jnp.where(both, j // 2, lax.rem(j, nc))
+
+    def at_step(s, lag):
+        n = s - lag
+        layer = jnp.maximum(n, 0) // steps
+        j2 = n - layer * steps
+        return (n >= 0) & (layer < layers) & (j2 < 2 * used) & (lax.rem(jnp.maximum(j2, 0), 2) == 0), layer, j2 // 2
 
     def row_of(h, t):
         return pl.multiple_of(h * (nt * rows) + t * rows, rows)
@@ -264,9 +256,36 @@
             wd_send.at[layer, cc], wd_recv.at[layer, cc], x_peer,
         )
 
-    def send_gu(layer, cc):
-        gu_copy(layer, cc, 0).start()
-        gu_copy(layer, cc, 1).start()
+    per_layer = 3 * nc
+    n_messages = layers * per_layer
+
+    def message(w, act):
+        layer = w // per_layer
+        k = w - layer * per_layer
+        k2 = k - 2 * LEAD
+        k3 = k2 - 3 * (nc - LEAD)
+        m = jnp.maximum(k2, 0) // 3
+        turn = jnp.maximum(k2, 0) - 3 * m
+        early = k2 < 0
+        is_down = jnp.logical_not(early) & ((k3 >= 0) | (turn == 0))
+        which = jnp.where(early, lax.rem(k, 2), turn - 1)
+        gu_at = jnp.where(early, k // 2, LEAD + m)
+        d_at = jnp.where(k3 >= 0, nc - LEAD + k3, m)
+
+        @pl.when(is_down)
+        def _():
+            act(d_copy(layer, d_at))
+
+        for part_at in range(2):
+            @pl.when(jnp.logical_not(is_down) & (which == part_at))
+            def _(part_at=part_at):
+                act(gu_copy(layer, gu_at, part_at))
+
+    def issue(w):
+        message(w, lambda copy: copy.start())
+
+    def issued(w):
+        message(w, lambda copy: copy.wait_send())
 
     def own_gu(layer, cc, which):
         src = gate_hbm if which == 0 else up_hbm
@@ -297,14 +316,36 @@
         view = stream.at[mine, other_cols]
         return remote(view, view, cg_send.at[h, t], cg_recv.at[h, t], core_peer)
 
-    for t in range(nt):
+    soon = min(2, nt)
+    for t in range(soon):
         for h in range(2):
             first_x(h, t).start()
-        if t == 0:
-            own_x.start()
-            send_gu(0, 0)
-    for cc in range(1, min(IN_FLIGHT, nc)):
-        send_gu(0, cc)
+    own_x.start()
+    for w in range(AHEAD):
+        issue(jnp.int32(w))
+        if w == 1:
+            for t in range(soon, nt):
+                for h in range(2):
+                    first_x(h, t).start()
+
+    def pass_y(chunks):
+        for t in chunks:
+            for h in range(2):
+                first_x(h, t).wait_recv()
+                first_y(h, t).start()
+
+    def pass_core(chunks):
+        for t in chunks:
+            for h in range(2):
+                first_y(h, t).wait_recv()
+                first_core(h, t).start()
+
+    def passed(chunks):
+        for t in chunks:
+            for h in range(2):
+                first_x(h, t).wait_send()
+                first_y(h, t).wait_send()
+                first_core(h, t).wait_send()
 
     def own_start(j, _):
         layer, cc = j // nc, lax.rem(j, nc)
@@ -321,37 +362,29 @@
         return 0
 
     lax.fori_loop(0, layers * nc, own_start, 0)
-    for t in range(nt):
-        for h in range(2):
-            first_x(h, t).wait_recv()
-            first_y(h, t).start()
+    pass_y(range(soon))
     own_x.wait()
-    for t in range(nt):
-        for h in range(2):
-            first_y(h, t).wait_recv()
-            first_core(h, t).start()
+    pass_core(range(soon))
     lax.fori_loop(0, layers * nc, own_wait, 0)
-    for t in range(nt):
-        for h in range(2):
-            first_x(h, t).wait_send()
-            first_y(h, t).wait_send()
-            first_core(h, t).wait_send()
-
-    def sum_copy(h, n):
-        _, t, cc = order(n)
+    passed(range(soon))
+    for w in range(AHEAD - IN_FLIGHT):
+        issued(jnp.int32(w))
+
+    def sum_copy(h, layer, j):
+        t, cc = order(j)
         _, ahead, _ = place(h)
         view = sums.at[h, t * nc + cc]
-        return remote(view, view, sum_send.at[h, lax.rem(n, 4)], sum_recv.at[h, t * nc + cc], ahead)
-
-    def hid_copy(h, n):
-        _, t, cc = order(n)
+        return remote(view, view, sum_send.at[h, lax.rem(layer * used + j, 4)], sum_recv.at[h, t * nc + cc], ahead)
+
+    def hid_copy(h, layer, j):
+        t, cc = order(j)
         _, _, back = place(h)
         view = hid.at[h, t * nc + cc]
-        return remote(view, view, hid_send.at[h, lax.rem(n, 4)], hid_recv.at[h, t * nc + cc], back)
-
-    def stage_sum(h, n):
+        return remote(view, view, hid_send.at[h, lax.rem(layer * used + j, 4)], hid_recv.at[h, t * nc + cc], back)
+
+    def stage_sum(h, layer, j):
         p, _, _ = place(h)
-        layer, t, cc = order(n)
+        t, cc = order(j)
 
         @pl.when((cc == 0) & (layer == 0))
         def _():
@@ -359,7 +392,7 @@
 
         @pl.when((cc == 0) & (layer > 0))
         def _():
-            gather_core(h, t).wait_recv()
+            gather_core(h, t, False).wait_recv()
 
         slot = t * nc + cc
         own = jnp.dot(stream[pl.ds(row_of(h, t), rows), :], wgu[layer, cc], preferred_element_type=F32)
@@ -370,32 +403,32 @@
 
         @pl.when((p > 0) & (p < groups - 1))
         def _():
-            sum_copy(h, n).wait_recv()
+            sum_copy(h, layer, j).wait_recv()
             sums[h, slot] = (sums[h, slot].astype(F32) + own).astype(BF16)
 
         @pl.when(p < groups - 1)
         def _():
-            sum_copy(h, n).start()
+            sum_copy(h, layer, j).start()
 
         @pl.when(p == groups - 1)
         def _():
-            sum_copy(h, n).wait_recv()
+            sum_copy(h, layer, j).wait_recv()
             whole = sums[h, slot].astype(F32) + own
             hid[h, slot] = (jax.nn.silu(whole[:, :UNIT]) * whole[:, UNIT:]).astype(BF16)
 
-    def stage_hid(h, n):
+    def stage_hid(h, layer, j):
         p, _, _ = place(h)
 
         @pl.when(p < groups - 1)
         def _():
-            hid_copy(h, n).wait_recv()
+            hid_copy(h, layer, j).wait_recv()
 
         @pl.when(p > 0)
         def _():
-            hid_copy(h, n).start()
-
-    def stage_down(h, n):
-        layer, t, cc = order(n)
+            hid_copy(h, layer, j).start()
+
+    def stage_down(h, layer, j):
+        t, cc = order(j)
         part_sum = jnp.dot(hid[h, t * nc + cc], wd[layer, cc], preferred_element_type=F32)
         m = h * nt + t
 
@@ -411,29 +444,26 @@
         m = h * nt + t
         return remote(core_out.at[m], core_in.at[m], core_send.at[h, t], core_recv.at[h, t], core_peer)
 
-    def y_copy(h, t):
+    def plane_copy(h, t, k):
         m = h * nt + t
-        return remote(y_out.at[m], y_in.at[m], y_send.at[h, t], y_recv.at[h, t], y_peer)
-
-    def x_copy(h, t):
-        m = h * nt + t
-        return remote(x_out.at[m], x_in.at[m], x_send.at[h, t], x_recv.at[h, t], x_peer)
+        return remote(
+            plane_out.at[m, k], plane_in.at[m, k], plane_send.at[h, t, k], plane_recv.at[h, t, k], (x_peer, y_peer, far_peer)[k]
+        )
 
     def stat_copy(h, t, k):
         m = h * nt + t
         return remote(stat_out.at[m], stat_in.at[m, k], stat_send.at[h, t, k], stat_recv.at[h, t, k], (lax.rem(r + k, n_ra), c))
 
-    def gather_x(h, t):
+    def gather_plane(h, t, k):
         mine = rows_at(row_of(h, t) + core * half_rows + y * quarter, quarter)
-        return remote(stream.at[mine, pl.ds(0, width)], stream.at[mine, other_cols], xg_send.at[h, t], xg_recv.at[h, t], x_peer)
-
-    def gather_y(h, t):
-        mine = rows_at(row_of(h, t) + core * half_rows + y * quarter, quarter)
-        return remote(stream.at[mine, :], stream.at[mine, :], yg_send.at[h, t], yg_recv.at[h, t], y_peer)
-
-    def gather_core(h, t):
+        lands = stream.at[mine, pl.ds(0, width) if k == 1 else other_cols]
+        send, recv = ((xg_send, xg_recv), (yg_send, yg_recv), (dg_send, dg_recv))[k]
+        return remote(stream.at[mine, pl.ds(0, width)], lands, send.at[h, t], recv.at[h, t], (x_peer, y_peer, far_peer)[k])
+
+    def gather_core(h, t, last):
         mine = rows_at(row_of(h, t) + core * half_rows, half_rows)
-        return remote(stream.at[mine, :], stream.at[mine, :], cg_send.at[h, t], cg_recv.at[h, t], core_peer)
+        cols = pl.ds(0, width) if last else pl.ds(0, 2 * width)
+        return remote(stream.at[mine, cols], stream.at[mine, cols], cg_send.at[h, t], cg_recv.at[h, t], core_peer)
 
     def out_copy(h, t):
         at = pl.ds(row_of(h, t), rows)
@@ -449,19 +479,16 @@
         core_out[m] = acc[m, pl.ds(sent_half, half_rows), :].astype(BF16)
         core_copy(h, t).start()
 
-    def end_y(h, layer, t):
+    def end_plane(h, layer, t):
         m = h * nt + t
         core_copy(h, t).wait()
         acc[m, pl.ds(kept_half, half_rows), :] += core_in[m].astype(F32)
-        y_out[m] = acc[m, pl.ds(sent, quarter), :].astype(BF16)
-        y_copy(h, t).start()
-
-    def end_x(h, layer, t):
-        m = h * nt + t
-        y_copy(h, t).wait()
-        acc[m, pl.ds(kept, quarter), :] += y_in[m].astype(F32)
-        x_out[m] = acc[m, pl.ds(kept, quarter), pl.ds(width, width)].astype(BF16)
-        x_copy(h, t).start()
+        plane_out[m, 2] = acc[m, pl.ds(sent, quarter), pl.ds(width, width)].astype(BF16)
+        plane_copy(h, t, 2).start()
+        plane_out[m, 0] = acc[m, pl.ds(kept, quarter), pl.ds(width, width)].astype(BF16)
+        plane_copy(h, t, 0).start()
+        plane_out[m, 1] = acc[m, pl.ds(sent, quarter), pl.ds(0, width)].astype(BF16)
+        plane_copy(h, t, 1).start()
 
     def lane_fold(v):
         total_v = v[:, :UNIT]
@@ -474,8 +501,10 @@
 
     def end_stats(h, layer, t):
         m = h * nt + t
-        x_copy(h, t).wait()
-        branch = acc[m, pl.ds(kept, quarter), pl.ds(0, width)] + x_in[m].astype(F32)
+        branch = acc[m, pl.ds(kept, quarter), pl.ds(0, width)]
+        for k in range(3):
+            plane_copy(h, t, k).wait()
+            branch = branch + plane_in[m, k].astype(F32)
         mine = stream[rows_at(row_of(h, t) + kept, quarter), pl.ds(0, width)]
         mixed = RESIDUAL * mine.astype(F32) + branch
         acc[m, pl.ds(kept, quarter), pl.ds(0, width)] = mixed
@@ -504,180 +533,163 @@
 
         @pl.when(layer < layers - 1)
         def _():
-            gather_x(h, t).start()
-
-    def end_gather_y(h, layer, t):
+            gather_plane(h, t, 2).start()
+            gather_plane(h, t, 0).start()
+
+        gather_plane(h, t, 1).start()
+
+    def end_gather_core(h, layer, t):
         @pl.when(layer < layers - 1)
         def _():
-            gather_x(h, t).wait()
-
-        gather_y(h, t).start()
-
-    def end_gather_core(h, layer, t):
-        gather_y(h, t).wait()
-        gather_core(h, t).start()
+            for k in range(3):
+                gather_plane(h, t, k).wait()
+            gather_core(h, t, False).start()
+
+        @pl.when(layer == layers - 1)
+        def _():
+            gather_plane(h, t, 1).wait()
+            gather_core(h, t, True).start()
 
     def end_sent(h, layer, t):
-        gather_core(h, t).wait_send()
+        @pl.when(layer < layers - 1)
+        def _():
+            gather_core(h, t, False).wait_send()
 
         @pl.when(layer == layers - 1)
         def _():
-            gather_core(h, t).wait_recv()
+            gather_core(h, t, True).wait()
             out_copy(h, t).start()
 
-    longest = HOP * 2 * (groups - 1)
+    longest = (HOP + BACK) * (groups - 1)
+
+    def lag_sum(h):
+        return HOP * place(h)[0]
 
     def lag_hid(h):
-        return longest - HOP * place(h)[0]
+        return longest - BACK * place(h)[0]
 
     stages = (
         (lambda h: lag_hid(h), end_core),
-        (lambda h: lag_hid(h) + ENDS[0], end_y),
-        (lambda h: lag_hid(h) + ENDS[1], end_x),
-        (lambda h: lag_hid(h) + ENDS[2], end_stats),
-        (lambda h: longest + ENDS[3], end_norm),
-        (lambda h: longest + ENDS[4], end_gather_y),
-        (lambda h: longest + ENDS[5], end_gather_core),
-        (lambda h: longest + ENDS[6], end_sent),
+        (lambda h: lag_hid(h) + ENDS[0], end_plane),
+        (lambda h: lag_hid(h) + ENDS[1], end_stats),
+        (lambda h: longest + ENDS[2], end_norm),
+        (lambda h: longest + ENDS[3], end_gather_core),
+        (lambda h: longest + ENDS[4], end_sent),
     )
 
     p0, p1 = place(0)[0], place(1)[0]
     p_low, p_high = jnp.minimum(p0, p1), jnp.maximum(p0, p1)
 
-    def weight_message(w):
-        layer = w // (2 * nc)
-        k = w - layer * 2 * nc
-        lead = jnp.where(layer == 0, IN_FLIGHT, 1)
-        mid = k - lead
-        in_mid = (mid >= 0) & (mid < 2 * (nc - lead))
-        is_gu = (k < lead) | (in_mid & (lax.rem(jnp.maximum(mid, 0), 2) == 1))
-        gu_at = jnp.where(k < lead, k, lead + mid // 2)
-        d_at = jnp.where(in_mid, mid // 2, k - nc)
-        return layer, is_gu, gu_at, d_at
-
-    n_messages = 2 * nc * layers
-
-    def issue_weights(w):
-        layer, is_gu, gu_at, d_at = weight_message(w)
-
-        @pl.when(is_gu)
-        def _():
-            send_gu(layer, gu_at)
-
-        @pl.when(jnp.logical_not(is_gu))
-        def _():
-            d_copy(layer, d_at).start()
-
-    def sent_weights(w):
-        layer, is_gu, gu_at, d_at = weight_message(w)
-
-        @pl.when(is_gu)
-        def _():
-            gu_copy(layer, gu_at, 0).wait_send()
-            gu_copy(layer, gu_at, 1).wait_send()
-
-        @pl.when(jnp.logical_not(is_gu))
-        def _():
-            d_copy(layer, d_at).wait_send()
-
-    fast = 2 * nc - IN_FLIGHT
-
-    def body(i, _):
-        j = i - fast
-        slow = (j >= 0) & (lax.rem(jnp.maximum(j, 0), 5) < 4)
-        w = jnp.where(j < 0, IN_FLIGHT + i, 2 * nc + (j // 5) * 4 + lax.rem(jnp.maximum(j, 0), 5))
-
-        @pl.when(((j < 0) | slow) & (w < n_messages))
-        def _():
-            sent_weights(w - IN_FLIGHT)
-            issue_weights(w)
-
-        n_w = i - HOP * p_low
-        layer_w, t_w, c_w = order(n_w)
-
-        @pl.when(valid(n_w) & (t_w == 0))
+    first_layer = -(-(per_layer - AHEAD) // 3) * EARLY_OF
+
+    def body(s, _):
+        late = jnp.maximum(s - first_layer, 0)
+        early = s < first_layer
+        turn = jnp.where(early, lax.rem(s, EARLY_OF), lax.rem(late, LATE_OF))
+        w = jnp.where(early, AHEAD + (s // EARLY_OF) * 3, per_layer + (late // LATE_OF) * 3) + turn
+        most = jnp.where(early, per_layer, n_messages)
+
+        @pl.when((turn < 3) & (w < most))
+        def _():
+            issued(w - IN_FLIGHT)
+            issue(w)
+
+        for step, act in zip(LATE, (pass_y, pass_core, passed)):
+            @pl.when(s == step)
+            def _(act=act):
+                act(range(soon, nt))
+
+        ok, layer_w, j_w = at_step(s, HOP * p_low)
+        t_w, c_w = order(j_w)
+
+        @pl.when(ok & (t_w == 0))
         def _():
             gu_copy(layer_w, c_w, 0).wait_recv()
             gu_copy(layer_w, c_w, 1).wait_recv()
 
-        n_d = i - longest + HOP * p_high
-        layer_d, t_d, c_d = order(n_d)
-
-        @pl.when(valid(n_d) & (t_d == 0))
+        ok, layer_d, j_d = at_step(s, longest - BACK * p_high)
+        t_d, c_d = order(j_d)
+
+        @pl.when(ok & (t_d == 0))
         def _():
             d_copy(layer_d, c_d).wait_recv()
 
         for h in range(2):
             p, _, _ = place(h)
-            n_s = i - HOP * p
-            n_h = i - lag_hid(h)
-
-            @pl.when(valid(n_s - 2) & (p < groups - 1))
-            def _(h=h, n=n_s - 2):
-                sum_copy(h, n).wait_send()
-
-            @pl.when(valid(n_h - 2) & (p > 0))
-            def _(h=h, n=n_h - 2):
-                hid_copy(h, n).wait_send()
-
-            @pl.when(valid(n_h) & (p < groups - 1))
-            def _(h=h, n=n_h):
-                stage_hid(h, n)
+            ok, layer, j = at_step(s, lag_sum(h) + SENT)
+
+            @pl.when(ok & (p < groups - 1))
+            def _(h=h, layer=layer, j=j):
+                sum_copy(h, layer, j).wait_send()
+
+            ok, layer, j = at_step(s, lag_hid(h) + SENT)
+
+            @pl.when(ok & (p > 0))
+            def _(h=h, layer=layer, j=j):
+                hid_copy(h, layer, j).wait_send()
+
+            ok, layer, j = at_step(s, lag_hid(h))
+
+            @pl.when(ok & (p < groups - 1))
+            def _(h=h, layer=layer, j=j):
+                stage_hid(h, layer, j)
 
         for h in range(2):
             p, _, _ = place(h)
-            n_s = i - HOP * p
-
-            @pl.when(valid(n_s))
-            def _(h=h, n=n_s):
-                stage_sum(h, n)
-
-            @pl.when(valid(n_s) & (p == groups - 1))
-            def _(h=h, n=n_s):
-                stage_hid(h, n)
+            ok, layer, j = at_step(s, lag_sum(h))
+
+            @pl.when(ok)
+            def _(h=h, layer=layer, j=j):
+                stage_sum(h, layer, j)
+
+            @pl.when(ok & (p == groups - 1))
+            def _(h=h, layer=layer, j=j):
+                stage_hid(h, layer, j)
 
         for h in range(2):
-            n_h = i - lag_hid(h)
-
-            @pl.when(valid(n_h))
-            def _(h=h, n=n_h):
-                stage_down(h, n)
+            ok, layer, j = at_step(s, lag_hid(h))
+
+            @pl.when(ok)
+            def _(h=h, layer=layer, j=j):
+                stage_down(h, layer, j)
 
         for lag, stage in stages:
             for h in range(2):
-                n_e = i - lag(h)
-                layer_e, t_e, c_e = order(n_e)
-
-                @pl.when(valid(n_e) & (c_e == nc - 1))
-                def _(h=h, stage=stage, layer_e=layer_e, t_e=t_e):
-                    stage(h, layer_e, t_e)
+                ok, layer, j = at_step(s, lag(h))
+
+                @pl.when(ok)
+                def _(h=h, stage=stage, layer=layer, j=j):
+                    t, cc = order(j)
+
+                    @pl.when(cc == nc - 1)
+                    def _():
+                        stage(h, layer, t)
 
         return 0
 
-    lax.fori_loop(0, total + longest + ENDS[6], body, 0)
+    lax.fori_loop(0, layers * steps + longest + ENDS[4], body, 0)
     for w in range(n_messages - IN_FLIGHT, n_messages):
-        sent_weights(jnp.int32(w))
+        issued(jnp.int32(w))
     for t in range(nt):
         for h in range(2):
             out_copy(h, t).wait()
 
 
-ENDS = (1, 3, 5, 7, 9, 11, 12)
+ENDS = (1, 4, 6, 9, 10)
 
 
 def layer_gap(groups, nc, nt):
-    after = HOP * 2 * (groups - 1) + ENDS[5] + 1
-    pairs = nc // 2
-    ends = [2 * pairs + pairs - 2 if nc == 2 * pairs else 3 * pairs]
-    ends += [3 * pairs + (nc - 2 * pairs) + (nc - pairs) - 1]
-    ends += [t * nc + nc - 1 for t in range(2, nt)]
-    return max([0] + [ends[t] + after - (nc * nt + t * nc) for t in range(nt)])
+    after = (HOP + BACK) * (groups - 1) + ENDS[3] + 1
+    ends = [2 * nc - 2, 2 * nc - 1] + [t * nc + nc - 1 for t in range(2, nt)]
+    starts = [0, 1] + [t * nc for t in range(2, nt)]
+    gap = max([0] + [2 * (ends[t] - starts[t] - nc * nt) + after for t in range(nt)])
+    return gap
 
 
 def fits(ra, cb, tokens, width, columns):
     units = columns // PAIR
     return (
-        ra % PAIR == 0 and ra >= 2 * PAIR and cb == 4 and units % UNIT == 0 and units // UNIT > IN_FLIGHT
+        ra % PAIR == 0 and ra >= 2 * PAIR and cb == 4 and units % UNIT == 0 and units // UNIT > AHEAD
         and width % UNIT == 0 and tokens % (2 * TOKEN_PARTS * 4 * 16) == 0
     )
 
@@ -700,18 +712,16 @@
         pltpu.VMEM((chunks, rows, 2 * width), F32),
         pltpu.VMEM((chunks, rows // 2, 2 * width), BF16),
         pltpu.VMEM((chunks, rows // 2, 2 * width), BF16),
-        pltpu.VMEM((chunks, rows // 4, 2 * width), BF16),
-        pltpu.VMEM((chunks, rows // 4, 2 * width), BF16),
-        pltpu.VMEM((chunks, rows // 4, width), BF16),
-        pltpu.VMEM((chunks, rows // 4, width), BF16),
+        pltpu.VMEM((chunks, 3, rows // 4, width), BF16),
+        pltpu.VMEM((chunks, 3, rows // 4, width), BF16),
         pltpu.VMEM((chunks, 8, rows // 4), F32),
         pltpu.VMEM((chunks, ra, 8, rows // 4), F32),
         dma((2, layers, nc, 2)),
         dma((layers, nc, 2)), dma((layers, nc, 2)), dma((layers, nc)), dma((layers, nc)),
         dma((2, 4)), dma((2, slots)), dma((2, 4)), dma((2, slots)),
-        dma((2, nt)), dma((2, nt)), dma((2, nt)), dma((2, nt)), dma((2, nt)), dma((2, nt)),
+        dma((2, nt)), dma((2, nt)), dma((2, nt, 3)), dma((2, nt, 3)),
         dma((2, nt, ra)), dma((2, nt, ra)),
-        dma((2, nt)), dma((2, nt)), dma((2, nt)), dma((2, nt)), dma((2, nt)), dma((2, nt)),
+        dma((2, nt)), dma((2, nt)), dma((2, nt)), dma((2, nt)), dma((2, nt)), dma((2, nt)), dma((2, nt)), dma((2, nt)),
         dma((1 + chunks,)),
     ]
     anywhere, near = pl.BlockSpec(memory_space=pl.ANY), pl.BlockSpec(memory_space=pltpu.VMEM)

time: 399 us -> 376 us (0.942)
  Pallas kernels: 396 us -> 373 us
    pallas_call x1, Pallas kernels: 396 us -> 373 us  [per_device_kernel(): pl.pallas_call(functools.partial(layer_kernel, groups), out_shape=jax.Sha...]
where the time goes in v2:
time: 376 us; the launch traced here: 375 us
  Pallas kernels  373 us (99%)
    pallas_call x1, Pallas kernels, per_device_kernel(): pl.pallas_call(functools.partial(layer_kernel, groups), out_shape=jax.Sha...  373 us

profile of v2, /device:TPU:0, one launch (start us, length us, event | category | flops | bytes accessed | tf_op | source)
XLA Modules:
  0.0 375.4 jit_solution(16803751372919026335)
XLA Ops:
  0.0 372.7 %shard_map.64 = bf16[1536,512]{1,0:T(8,128)(2,1)} custom-call(bf16[1536,512]{1,0:T(8,128)(2,1)} %x_hbm.1, bf16[2,512,2816]{2,1,0:T(8,128)(2,1)} %gate_hbm.1, bf16[2,512,2816]{2,1,0:T(8,128)(2,1)} %up_hbm.1, bf16[2,2816,512]{2,1,0:T(8,128)(2,1)} %down_hbm.1, f32[2,512]{1,0:T(2,128)} %gain.1, f32[2,512]{1,0:T(2,128)} %shift.1), custom_call_target="tpu_custom_call" | custom-call | tf_op jit(solution)/shard_map/pallas_call | solution.py:728
  372.7 2.7 copy.8

commit v3 on v2

--- a/solution.py
+++ b/solution.py
@@ -179,9 +179,9 @@
 HOP = 3
 BACK = 3
 SENT = 4
-LEAD = 2
-AHEAD = 6
-IN_FLIGHT = 4
+LEAD = 5
+AHEAD = 10
+IN_FLIGHT = 8
 EARLY_OF = 4
 LATE_OF = 7
 LATE = (6, 10, 14)

time: 376 us -> 373 us (level)
  no operation moved by 1% of the time
where the time goes in v3:
time: 373 us
  Pallas kernels  370 us (99%)
    pallas_call x1, Pallas kernels, per_device_kernel(): pl.pallas_call(functools.partial(layer_kernel, groups), out_shape=jax.Sha...  370 us

profile of v3, /device:TPU:0, one launch (start us, length us, event | category | flops | bytes accessed | tf_op | source)
XLA Modules:
  0.0 372.6 jit_solution(3403891668283338309)
XLA Ops:
  0.0 370.0 %shard_map.64 = bf16[1536,512]{1,0:T(8,128)(2,1)} custom-call(bf16[1536,512]{1,0:T(8,128)(2,1)} %x_hbm.1, bf16[2,512,2816]{2,1,0:T(8,128)(2,1)} %gate_hbm.1, bf16[2,512,2816]{2,1,0:T(8,128)(2,1)} %up_hbm.1, bf16[2,2816,512]{2,1,0:T(8,128)(2,1)} %down_hbm.1, f32[2,512]{1,0:T(2,128)} %gain.1, f32[2,512]{1,0:T(2,128)} %shift.1), custom_call_target="tpu_custom_call" | custom-call | tf_op jit(solution)/shard_map/pallas_call | solution.py:728
  370.0 2.7 copy.8
